TPU v7x, 32 devices: a whole 2x2x4 slice. The times are simulated.
32 devices in a mesh: ep: 16 (over z, y, x), tp: 2 (over core).
Axes of the slice: x: 2, y: 2, z: 4, core: 2. Of those that a mesh axis runs over, the one named last changes fastest.
Arguments:
- tokens: bfloat16 [512, 2048], P('ep'), may hold values from -6 to 6
- mix_gain: float32 [2048], replicated, may hold values from 0.1 to 1.9
- w_query: bfloat16 [2048, 512], P('ep', 'tp'), may hold values from -0.125 to 0.125
- w_key: bfloat16 [2048, 512], P('ep', 'tp'), may hold values from -0.125 to 0.125
- w_value: bfloat16 [2048, 512], P('ep', 'tp'), may hold values from -0.125 to 0.125
- w_outgate: bfloat16 [2048, 512], P('ep', 'tp'), may hold values from -0.125 to 0.125
- w_igate: bfloat16 [2048, 8], P('ep', 'tp'), may hold values from -0.125 to 0.125
- w_fgate: bfloat16 [2048, 8], P('ep', 'tp'), may hold values from -0.125 to 0.125
- igate_bias: float32 [8], P('tp'), may hold values from -2 to 1
- fgate_bias: float32 [8], P('tp'), may hold values from 0 to 4
- head_gain: float32 [512], P('tp'), may hold values from 0.1 to 1.9
- w_out: bfloat16 [512, 2048], P('tp', 'ep'), may hold values from -0.25 to 0.25
- state_matrix: float32 [512, 8, 64, 64], P('ep', 'tp'), may hold values from -2.4 to 2.4
- state_norm: float32 [512, 8, 64], P('ep', 'tp'), may hold values from -2.4 to 2.4
- state_max: float32 [512, 8], P('ep', 'tp'), may hold values from -4 to 4
- ffn_gain: float32 [2048], replicated, may hold values from 0.1 to 1.9
- w_expert_gate: bfloat16 [16, 2048, 1408], P('ep', None, 'tp'), may hold values from -0.125 to 0.125
- w_expert_up: bfloat16 [16, 2048, 1408], P('ep', None, 'tp'), may hold values from -0.125 to 0.125
- w_expert_down: bfloat16 [16, 1408, 2048], P('ep', 'tp'), may hold values from -0.15625 to 0.15625
- routes: int32 [512, 3], P('ep'), may hold values from 0 to 15, all different within a row; in each aligned block of 32 rows (0 to 31, 32 to 63, ...) at most 12 rows name the same one
- route_weights: float32 [512, 3], P('ep'), may hold values from 0.2 to 1
Outputs:
- mixed: bfloat16 [512, 2048], P('ep')
- new_matrix: float32 [512, 8, 64, 64], P('ep', 'tp')
- new_norm: float32 [512, 8, 64], P('ep', 'tp')
- new_max: float32 [512, 8], P('ep', 'tp')
Inputs may be any that keep to these rules, and one draw needn't show every extreme that they name: `routes`: each row names 3 different experts. Among the rows of one device, no expert is named by more than 12 rows, a bound that some block reaches.
All inputs are finite; a program needn't handle non-finite values.
Results may differ from a plain program's by a relative error of at most 0.017.
Values may be sent and summed in bfloat16 or wider, within the bound.
A program may use at most 128 MiB of HBM per device.

v0:
```python
import functools

import jax
import jax.numpy as jnp
from jax import lax
from jax.experimental import pallas as pl
from jax.experimental.pallas import tpu as pltpu
from jax.sharding import PartitionSpec as P

MESH = pl.DeviceIdType.MESH
PLANE = 4
LANES = 128
SLOT_TILE = 16
VMEM_BYTES = 60 * 1024 * 1024


def remote(src, dst, send_sem, recv_sem, target):
    return pltpu.make_async_remote_copy(
        src_ref=src,
        dst_ref=dst,
        send_sem=send_sem,
        recv_sem=recv_sem,
        device_id=target,
        device_id_type=MESH,
    )


def dot_t(left, right):
    return lax.dot_general(
        left, right, (((1,), (1,)), ((), ())), preferred_element_type=jnp.float32
    )


def fetch_all(pairs, sems):
    copies = []
    for index, (source, kept) in enumerate(pairs):
        copy = pltpu.make_async_copy(source, kept, sems.at[index])
        copy.start()
        copies.append(copy)
    return copies


def mixer_kernel(
    lines,
    tokens_hbm,
    gain_hbm,
    wq_ref,
    wk_ref,
    wv_ref,
    wo_gate_ref,
    igate_hbm,
    fgate_hbm,
    w_out_hbm,
    proj_ref,
    w_all_ref,
    tokens_ref,
    gain_ref,
    igate_ref,
    fgate_ref,
    turned,
    w_planes,
    normed,
    spread,
    weights,
    partial,
    outgoing,
    arrived,
    local_sem,
    w_send,
    w_recv,
    x_send,
    x_recv,
    p_send,
    p_recv,
    z_send,
    z_recv,
    o_send,
    o_recv,
):
    ep, tp = lax.axis_index("ep"), lax.axis_index("tp")
    line, spot = ep // PLANE, ep % PLANE
    rows, width = tokens_ref.shape
    depth = wq_ref.shape[0]
    block = depth * PLANE
    heads = igate_ref.shape[0]
    beside = spot + 1 - 2 * (spot % 2)
    across = lax.rem(spot + 2, PLANE)
    beside_peer = (line * PLANE + beside, tp)
    across_peer = (line * PLANE + across, tp)

    def line_peer(step):
        other = lax.rem(line + step, lines)
        return other, (other * PLANE + spot, tp)

    own_rows = pl.ds(pl.multiple_of(spot * depth, depth), depth)
    pairs = [
        (tokens_hbm, tokens_ref),
        (gain_hbm, gain_ref),
        (igate_hbm, igate_ref),
        (fgate_hbm, fgate_ref),
        (w_out_hbm, w_planes.at[spot, line]),
    ]
    start = 0
    for ref in (wq_ref, wk_ref, wv_ref, wo_gate_ref):
        columns = ref.shape[1]
        pairs.append((ref, weights.at[own_rows, start : start + columns]))
        start += columns
    main = start
    copies = fetch_all(pairs, local_sem)
    barrier = pltpu.get_barrier_semaphore()
    for step in range(1, lines):
        pl.semaphore_signal(barrier, inc=1, device_id=line_peer(step)[1], device_id_type=MESH)
    pl.semaphore_signal(barrier, inc=1, device_id=beside_peer, device_id_type=MESH)
    pl.semaphore_signal(barrier, inc=1, device_id=across_peer, device_id_type=MESH)
    turned[...] = jnp.zeros_like(turned)
    for copy in copies:
        copy.wait()
    for place in (0, LANES // 2):
        turned[place : place + heads, :] = igate_ref[...].astype(jnp.float32)
        turned[place + heads : place + 2 * heads, :] = fgate_ref[...].astype(jnp.float32)
    weights[own_rows, main:] = turned[...].T.astype(jnp.bfloat16)
    widened = tokens_ref[...].astype(jnp.float32)
    scale = lax.rsqrt(jnp.mean(widened * widened, axis=-1, keepdims=True) + 1e-06)
    normed[...] = (widened * scale * gain_ref[...]).astype(jnp.bfloat16)
    pl.semaphore_wait(barrier, lines - 1 + 2)

    def row_part(owner, part):
        size = depth // 2
        return pl.ds(pl.multiple_of(owner * depth + part * size, size), size)

    def w_copy(owner, part, slot, target):
        view = weights.at[row_part(owner, part)]
        return remote(view, view, w_send.at[slot], w_recv.at[slot], target)

    def o_copy(owner, part, slot, target):
        size = lines // 2
        view = w_planes.at[owner, part * size : part * size + size]
        return remote(view, view, o_send.at[slot], o_recv.at[slot], target)

    def open_plane(make):
        first = [
            make(spot, 0, 0, beside_peer),
            make(spot, 1, 2, across_peer),
            make(spot, 1, 1, beside_peer),
            make(spot, 0, 3, across_peer),
        ]
        for copy in first:
            copy.start()
        return first

    def relay_plane(make, first):
        first[0].wait_recv()
        ahead = make(beside, 0, 4, across_peer)
        ahead.start()
        first[1].wait_recv()
        aside = make(across, 1, 5, beside_peer)
        aside.start()
        return [ahead, aside]

    def close_plane(first, second):
        first[2].wait_recv()
        first[3].wait_recv()
        for copy in first:
            copy.wait_send()
        for copy in second:
            copy.wait()

    w_first = open_plane(w_copy)
    x_copies, z_copies, p_copies = [], [], []
    for step in range(1, lines):
        other, target = line_peer(step)
        copy = remote(
            normed.at[:, pl.ds(pl.multiple_of(other * block, block), block)],
            spread.at[line],
            x_send.at[step],
            x_recv.at[step],
            target,
        )
        copy.start()
        x_copies.append(copy)
    for step in range(1, lines):
        own = w_planes.at[spot, line]
        copy = remote(own, own, z_send.at[step], z_recv.at[step], line_peer(step)[1])
        copy.start()
        z_copies.append(copy)
    spread[line] = normed[:, pl.ds(pl.multiple_of(line * block, block), block)]
    w_second = relay_plane(w_copy, w_first)
    for copy in z_copies:
        copy.wait()
    o_first = open_plane(o_copy)
    for copy in x_copies:
        copy.wait()
    close_plane(w_first, w_second)
    product = jnp.dot(
        spread[...].reshape(lines * rows, block),
        weights[...],
        preferred_element_type=jnp.float32,
    )
    outgoing[:, :, :main] = product[:, :main].astype(jnp.bfloat16).reshape(lines, rows, main)
    gates = product[:, main:]
    coarse = gates.astype(jnp.bfloat16)
    fine = (gates - coarse.astype(jnp.float32)).astype(jnp.bfloat16)
    first = lax.broadcasted_iota(jnp.int32, gates.shape, 1) < LANES // 2
    picked = jnp.where(first, coarse.astype(jnp.float32), fine.astype(jnp.float32))
    outgoing[:, :, main:] = picked.astype(jnp.bfloat16).reshape(lines, rows, LANES)
    partial[:, :, :main] = product[:, :main].reshape(lines, rows, main)
    partial[:, :, main:] = jnp.where(first, gates, 0.0).reshape(lines, rows, LANES)
    for step in range(1, lines):
        other, target = line_peer(step)
        copy = remote(
            outgoing.at[other], arrived.at[step], p_send.at[step], p_recv.at[step], target
        )
        copy.start()
        p_copies.append(copy)
    o_second = relay_plane(o_copy, o_first)
    total = partial[line]
    for step in range(1, lines):
        p_copies[step - 1].wait()
        total = total + arrived[step].astype(jnp.float32)
    proj_ref[...] = total
    close_plane(o_first, o_second)
    store = pltpu.make_async_copy(w_planes, w_all_ref, local_sem.at[0])
    store.start()
    store.wait()


def cell_kernel(
    proj_ref,
    ibias_hbm,
    fbias_hbm,
    head_gain_hbm,
    matrix_hbm,
    norm_hbm,
    max_hbm,
    cell_ref,
    new_matrix_ref,
    new_norm_ref,
    new_max_ref,
    ibias_ref,
    fbias_ref,
    head_gain_ref,
    matrix,
    state_norm,
    state_max,
    turned,
    decay,
    left,
    keys,
    queries,
    reads,
    sems,
    in_sems,
    out_sems,
):
    rows, heads, size, _ = matrix.shape
    wide = heads * size
    pack = 2 * heads
    chunk = 8
    chunks = rows // chunk
    loads = []
    for index in range(chunks):
        part = pl.ds(index * chunk, chunk)
        copy = pltpu.make_async_copy(matrix_hbm.at[part], matrix.at[part], in_sems.at[index])
        copy.start()
        loads.append(copy)
    small = fetch_all(
        (
            (ibias_hbm, ibias_ref),
            (fbias_hbm, fbias_ref),
            (head_gain_hbm, head_gain_ref),
            (norm_hbm, state_norm),
            (max_hbm, state_max),
        ),
        sems,
    )
    turned[...] = jnp.zeros_like(turned)
    gates = proj_ref[:, 4 * wide :]
    gates = gates + pltpu.roll(gates, LANES // 2, 1)
    forget = pltpu.roll(gates, LANES - heads, 1)
    for copy in small:
        copy.wait()
    turned[:heads, :rows] = state_max[...]
    old_max = turned[...].T[:rows]
    turned[...] = jnp.zeros_like(turned)
    turned[0:1, :heads] = ibias_ref[...]
    turned[1:2, :heads] = fbias_ref[...]
    input_pre = gates + turned[0:1, :]
    forget_pre = forget + turned[1:2, :]
    log_forget = jnp.minimum(forget_pre, 0.0) - jnp.log(1.0 + jnp.exp(-jnp.abs(forget_pre)))
    new_max = jnp.maximum(log_forget + old_max, input_pre)
    keep_old = jnp.exp(log_forget + old_max - new_max)
    keep_new = jnp.exp(input_pre - new_max)
    turned[:rows, :] = new_max
    new_max_ref[...] = turned[...].T[:heads, :rows]
    place = lax.broadcasted_iota(jnp.int32, (rows, pack, LANES), 1)
    lane = lax.broadcasted_iota(jnp.int32, (rows, pack, LANES), 2)
    chosen = (place == lane) | (place == lane + heads)

    def per_head(values):
        spread = jnp.broadcast_to(values[:, None, :], (rows, pack, LANES))
        return jnp.sum(
            jnp.where(chosen & (lane < heads), spread, 0.0), axis=-1, keepdims=True
        )

    old_scale = per_head(keep_old)
    new_scale = per_head(keep_new)
    floor = per_head(jnp.exp(-new_max))
    decay[...] = jnp.broadcast_to(old_scale, decay.shape)
    row = lax.broadcasted_iota(jnp.int32, (rows, pack, wide), 1)
    head = lax.broadcasted_iota(jnp.int32, (rows, pack, wide), 2) // size
    same = (row == head) | (row == head + heads)
    fold = (
        lax.broadcasted_iota(jnp.int32, (wide, size), 0) % size
        == lax.broadcasted_iota(jnp.int32, (wide, size), 1)
    ).astype(jnp.float32).astype(jnp.bfloat16)

    def rounded(index):
        return proj_ref[:, index * wide : (index + 1) * wide].astype(jnp.bfloat16).astype(jnp.float32)

    def split_heads(values):
        spread = jnp.broadcast_to(values[:, None, :], (rows, pack, wide))
        masked = jnp.where(same, spread, 0.0).reshape(rows * pack, wide).astype(jnp.bfloat16)
        return jnp.dot(masked, fold, preferred_element_type=jnp.float32).reshape(
            rows, pack, size
        )

    query = split_heads(rounded(0))
    key = split_heads(rounded(1)) * size ** (-0.5)
    value = jnp.broadcast_to(rounded(2)[:, None, :], (rows, pack, wide))
    value = jnp.where(same, value * new_scale, 0.0)
    coarse = value.astype(jnp.bfloat16).astype(jnp.float32)
    left[...] = jnp.where(row < heads, coarse, value - coarse)
    keys[...] = key
    queries[...] = query
    new_norm = old_scale[:, :heads] * state_norm[...] + (new_scale * key)[:, :heads]
    new_norm_ref[...] = new_norm
    divisor = jnp.sum(new_norm * query[:, :heads], axis=-1, keepdims=True)
    divisor = jnp.maximum(jnp.abs(divisor), floor[:, :heads])
    stores = []
    for index in range(chunks):
        loads[index].wait()

        @pl.loop(0, chunk // 4)
        def _(group):
            for inner in range(4):
                item = index * chunk + group * 4 + inner
                outer = lax.dot_general(
                    left[item].astype(jnp.bfloat16),
                    keys[item].astype(jnp.bfloat16),
                    (((0,), (0,)), ((), ())),
                    preferred_element_type=jnp.float32,
                ).reshape(heads, size, size)
                scale = decay[item][:heads][:, None, :]
                fresh = scale * matrix[item] + outer
                matrix[item] = fresh
                flat = fresh.reshape(wide, size)
                high = flat.astype(jnp.bfloat16)
                low = (flat - high.astype(jnp.float32)).astype(jnp.bfloat16)
                asked = queries[item].astype(jnp.bfloat16)
                reads[item] = dot_t(asked, high) + dot_t(asked, low)

        part = pl.ds(index * chunk, chunk)
        copy = pltpu.make_async_copy(matrix.at[part], new_matrix_ref.at[part], out_sems.at[index])
        copy.start()
        stores.append(copy)
    only = (row == head)[:, :heads]
    read = jnp.where(only, reads[:, :heads, :] / divisor, 0.0)
    mean = jnp.sum(read, axis=-1, keepdims=True) / size
    centered = jnp.where(only, read - mean, 0.0)
    variance = jnp.sum(centered * centered, axis=-1, keepdims=True) / size
    scaled = jnp.sum(centered * lax.rsqrt(variance + 1e-06), axis=1)
    cell_ref[...] = (scaled * head_gain_ref[...] * jax.nn.sigmoid(rounded(3))).astype(jnp.bfloat16)
    for copy in stores:
        copy.wait()


def expert_kernel(
    count,
    cell_hbm,
    w_all_hbm,
    tokens_hbm,
    gain_hbm,
    routes_hbm,
    route_weights_hbm,
    w_gate_hbm,
    w_up_hbm,
    w_down_hbm,
    mixed_ref,
    cell_ref,
    w_all_ref,
    tokens_ref,
    gain_ref,
    routes_ref,
    route_weights_ref,
    w_gate,
    w_up,
    w_down,
    mine,
    theirs,
    resid,
    outgoing,
    near,
    far,
    down_send,
    down_recv,
    finished,
    returned,
    last_send,
    last_recv,
    local_sem,
    t_send,
    t_recv,
    d_send,
    d_recv,
    f_send,
    f_recv,
    r_send,
    r_recv,
):
    ep, tp = lax.axis_index("ep"), lax.axis_index("tp")
    partner = (ep, 1 - tp)
    rows, width = tokens_ref.shape
    half = width // 2
    slots = count * SLOT_TILE
    top = route_weights_ref.shape[0]
    loads = fetch_all(
        (
            (cell_hbm, cell_ref),
            (w_all_hbm, w_all_ref),
            (tokens_hbm, tokens_ref),
            (gain_hbm, gain_ref),
            (routes_hbm, routes_ref),
            (route_weights_hbm, route_weights_ref),
            (w_gate_hbm, w_gate),
            (w_up_hbm, w_up),
            (w_down_hbm, w_down),
        ),
        local_sem,
    )
    barrier = pltpu.get_barrier_semaphore()
    for step in range(1, count):
        pl.semaphore_signal(
            barrier, inc=1, device_id=(lax.rem(ep + step, count), tp), device_id_type=MESH
        )
    pl.semaphore_signal(barrier, inc=1, device_id=partner, device_id_type=MESH)
    for copy in loads[:6]:
        copy.wait()
    loads = loads[6:]
    cell = cell_ref[...]
    columns = w_all_ref.shape[3]
    lines = w_all_ref.shape[1]
    for line in range(lines):
        for spot in range(PLANE):
            start = (line * PLANE + spot) * columns
            mine[:, start : start + columns] = jnp.dot(
                cell, w_all_ref[spot, line], preferred_element_type=jnp.float32
            ).astype(jnp.bfloat16)
    pl.semaphore_wait(barrier, count)
    swap = remote(mine, theirs, t_send.at[0], t_recv.at[0], partner)
    swap.start()
    slot_row = lax.broadcasted_iota(jnp.int32, (slots, rows), 0).astype(jnp.float32)
    expert = lax.broadcasted_iota(jnp.int32, (count, rows), 0).astype(jnp.float32)
    before = (
        lax.broadcasted_iota(jnp.int32, (rows, rows), 0)
        < lax.broadcasted_iota(jnp.int32, (rows, rows), 1)
    ).astype(jnp.float32)
    taken = jnp.zeros((count, 1), jnp.float32)
    dispatch = jnp.zeros((slots, rows), jnp.float32)
    combine = jnp.zeros((slots, rows), jnp.float32)
    for k in range(top):
        named = routes_ref[k : k + 1, :].astype(jnp.float32)
        match = jnp.where(expert == named, 1.0, 0.0)
        earlier = jnp.dot(match, before, preferred_element_type=jnp.float32) + taken
        taken = taken + jnp.sum(match, axis=1, keepdims=True)
        target = named * SLOT_TILE + jnp.sum(match * earlier, axis=0, keepdims=True)
        hit = slot_row == target
        dispatch += jnp.where(hit, 1.0, 0.0)
        combine += jnp.where(hit, route_weights_ref[k : k + 1, :], 0.0)
    dispatch = dispatch.astype(jnp.bfloat16)
    coarse = combine.astype(jnp.bfloat16)
    fine = (combine - coarse.astype(jnp.float32)).astype(jnp.bfloat16)
    swap.wait()
    summed = mine[...].astype(jnp.float32) + theirs[...].astype(jnp.float32)
    resid[...] = (tokens_ref[...].astype(jnp.float32) + summed).astype(jnp.bfloat16)
    widened = resid[...].astype(jnp.float32)
    scale = lax.rsqrt(jnp.mean(widened * widened, axis=-1, keepdims=True) + 1e-06)
    my_half = pl.ds(pl.multiple_of(tp * half, half), half)
    other_half = pl.ds(pl.multiple_of((1 - tp) * half, half), half)
    normed = (resid[:, my_half].astype(jnp.float32) * scale * gain_ref[:, my_half]).astype(
        jnp.bfloat16
    )
    outgoing[...] = (
        jnp.dot(dispatch, normed, preferred_element_type=jnp.float32)
        .astype(jnp.bfloat16)
        .reshape(count, SLOT_TILE, half)
    )
    sends = []
    for step in range(1, count):
        other = lax.rem(ep + step, count)
        copy = remote(
            outgoing.at[other], near.at[ep], d_send.at[step], d_recv.at[step], (other, tp)
        )
        copy.start()
        sends.append(copy)
    near[ep] = outgoing[ep]
    forwards = []
    for step in range(count):
        source = lax.rem(ep + count - step, count)
        if step > 0:
            sends[step - 1].wait()
        copy = remote(
            near.at[source] if step > 0 else outgoing.at[ep],
            far.at[source],
            f_send.at[step],
            f_recv.at[step],
            partner,
        )
        copy.start()
        forwards.append(copy)
    for copy in loads:
        copy.wait()
    near_rows = near[...].reshape(slots, half)
    gate_pre = dot_t(near_rows, w_gate[:, my_half])
    up_pre = dot_t(near_rows, w_up[:, my_half])
    for copy in forwards:
        copy.wait()
    far_rows = far[...].reshape(slots, half)
    gate_pre += dot_t(far_rows, w_gate[:, other_half])
    up_pre += dot_t(far_rows, w_up[:, other_half])
    hidden = (gate_pre * jax.nn.sigmoid(gate_pre) * up_pre).astype(jnp.bfloat16)
    down_send[...] = jnp.dot(
        hidden, w_down[:, other_half], preferred_element_type=jnp.float32
    ).astype(jnp.bfloat16)
    swap = remote(down_send, down_recv, t_send.at[1], t_recv.at[1], partner)
    swap.start()
    kept = jnp.dot(hidden, w_down[:, my_half], preferred_element_type=jnp.float32).astype(
        jnp.bfloat16
    )
    swap.wait()
    finished[...] = (
        (kept.astype(jnp.float32) + down_recv[...].astype(jnp.float32))
        .astype(jnp.bfloat16)
        .reshape(count, SLOT_TILE, half)
    )
    sends = []
    for step in range(1, count):
        other = lax.rem(ep + step, count)
        copy = remote(
            finished.at[other], returned.at[ep], r_send.at[step], r_recv.at[step], (other, tp)
        )
        copy.start()
        sends.append(copy)
    returned[ep] = finished[ep]
    for copy in sends:
        copy.wait()
    back = returned[...].reshape(slots, half)
    turn = (((0,), (0,)), ((), ()))
    weighted = lax.dot_general(
        coarse, back, turn, preferred_element_type=jnp.float32
    ) + lax.dot_general(fine, back, turn, preferred_element_type=jnp.float32)
    last_send[...] = (resid[:, my_half].astype(jnp.float32) + weighted).astype(jnp.bfloat16)
    swap = remote(last_send, last_recv, t_send.at[2], t_recv.at[2], partner)
    swap.start()
    mixed_ref[:, my_half] = last_send[...]
    swap.wait()
    mixed_ref[:, other_half] = last_recv[...]


def mixer_call(tokens, mix_gain, weight_list, w_out):
    rows, width = tokens.shape
    w_query, w_key, w_value, w_outgate, w_igate, w_fgate = weight_list
    depth, columns = w_query.shape
    lines = lax.axis_size("ep") // PLANE
    heads = w_igate.shape[1]
    total = 4 * columns + LANES
    vmem = pl.BlockSpec(memory_space=pltpu.VMEM)
    anywhere = pl.BlockSpec(memory_space=pl.ANY)
    dma = pltpu.SemaphoreType.DMA
    bf = jnp.bfloat16
    planes = (PLANE, lines) + w_out.shape
    return pl.pallas_call(
        functools.partial(mixer_kernel, lines),
        out_shape=(
            jax.ShapeDtypeStruct((rows, total), jnp.float32),
            jax.ShapeDtypeStruct(planes, bf),
        ),
        in_specs=[anywhere] * 9,
        out_specs=(vmem, anywhere),
        scratch_shapes=[
            pltpu.VMEM((rows, width), bf),
            pltpu.VMEM((1, width), jnp.float32),
            pltpu.VMEM((heads, depth), bf),
            pltpu.VMEM((heads, depth), bf),
            pltpu.VMEM((LANES, depth), jnp.float32),
            pltpu.VMEM(planes, bf),
            pltpu.VMEM((rows, width), bf),
            pltpu.VMEM((lines, rows, depth * PLANE), bf),
            pltpu.VMEM((depth * PLANE, total), bf),
            pltpu.VMEM((lines, rows, total), jnp.float32),
            pltpu.VMEM((lines, rows, total), bf),
            pltpu.VMEM((lines, rows, total), bf),
            dma((9,)),
            dma((6,)),
            dma((6,)),
            dma((lines,)),
            dma((lines,)),
            dma((lines,)),
            dma((lines,)),
            dma((lines,)),
            dma((lines,)),
            dma((6,)),
            dma((6,)),
        ],
        compiler_params=pltpu.CompilerParams(
            collective_id=0, has_side_effects=True, vmem_limit_bytes=VMEM_BYTES
        ),
    )(
        tokens,
        mix_gain[None, :],
        w_query,
        w_key,
        w_value,
        w_outgate,
        jnp.swapaxes(w_igate, 0, 1),
        jnp.swapaxes(w_fgate, 0, 1),
        w_out,
    )


def cell_call(proj, igate_bias, fgate_bias, head_gain, state_matrix, state_norm, state_max):
    rows, heads, size, _ = state_matrix.shape
    wide = heads * size
    vmem = pl.BlockSpec(memory_space=pltpu.VMEM)
    anywhere = pl.BlockSpec(memory_space=pl.ANY)
    dma = pltpu.SemaphoreType.DMA
    f32 = jnp.float32
    cell_out, new_matrix, new_norm, new_max = pl.pallas_call(
        cell_kernel,
        out_shape=(
            jax.ShapeDtypeStruct((rows, wide), jnp.bfloat16),
            jax.ShapeDtypeStruct(state_matrix.shape, f32),
            jax.ShapeDtypeStruct(state_norm.shape, f32),
            jax.ShapeDtypeStruct((heads, rows), f32),
        ),
        in_specs=[vmem] + [anywhere] * 6,
        out_specs=(vmem, anywhere, vmem, vmem),
        scratch_shapes=[
            pltpu.VMEM((1, heads), f32),
            pltpu.VMEM((1, heads), f32),
            pltpu.VMEM((1, wide), f32),
            pltpu.VMEM(state_matrix.shape, f32),
            pltpu.VMEM(state_norm.shape, f32),
            pltpu.VMEM((heads, rows), f32),
            pltpu.VMEM((LANES, LANES), f32),
            pltpu.VMEM((rows, 2 * heads, size), f32),
            pltpu.VMEM((rows, 2 * heads, wide), f32),
            pltpu.VMEM((rows, 2 * heads, size), f32),
            pltpu.VMEM((rows, 2 * heads, size), f32),
            pltpu.VMEM((rows, 2 * heads, wide), f32),
            dma((5,)),
            dma((rows // 8,)),
            dma((rows // 8,)),
        ],
        compiler_params=pltpu.CompilerParams(vmem_limit_bytes=VMEM_BYTES),
    )(
        proj,
        igate_bias[None, :],
        fgate_bias[None, :],
        head_gain[None, :],
        state_matrix,
        state_norm,
        jnp.swapaxes(state_max, 0, 1),
    )
    return cell_out, new_matrix, new_norm, jnp.swapaxes(new_max, 0, 1)


def expert_call(
    cell_out, w_all, tokens, ffn_gain, routes, route_weights, w_gate, w_up, w_down
):
    rows, width = tokens.shape
    count = lax.axis_size("ep")
    gate_t = jnp.swapaxes(w_gate[0], 0, 1)
    up_t = jnp.swapaxes(w_up[0], 0, 1)
    down = w_down[0]
    half = width // 2
    area = count * SLOT_TILE
    vmem = pl.BlockSpec(memory_space=pltpu.VMEM)
    anywhere = pl.BlockSpec(memory_space=pl.ANY)
    dma = pltpu.SemaphoreType.DMA
    bf = jnp.bfloat16
    tile = (count, SLOT_TILE, half)
    return pl.pallas_call(
        functools.partial(expert_kernel, count),
        out_shape=jax.ShapeDtypeStruct((rows, width), bf),
        in_specs=[anywhere] * 9,
        out_specs=vmem,
        scratch_shapes=[
            pltpu.VMEM(cell_out.shape, bf),
            pltpu.VMEM(w_all.shape, bf),
            pltpu.VMEM((rows, width), bf),
            pltpu.VMEM((1, width), jnp.float32),
            pltpu.VMEM((routes.shape[1], rows), jnp.int32),
            pltpu.VMEM((routes.shape[1], rows), jnp.float32),
            pltpu.VMEM(gate_t.shape, bf),
            pltpu.VMEM(up_t.shape, bf),
            pltpu.VMEM(down.shape, bf),
            pltpu.VMEM((rows, width), bf),
            pltpu.VMEM((rows, width), bf),
            pltpu.VMEM((rows, width), bf),
            pltpu.VMEM(tile, bf),
            pltpu.VMEM(tile, bf),
            pltpu.VMEM(tile, bf),
            pltpu.VMEM((area, half), bf),
            pltpu.VMEM((area, half), bf),
            pltpu.VMEM(tile, bf),
            pltpu.VMEM(tile, bf),
            pltpu.VMEM((rows, half), bf),
            pltpu.VMEM((rows, half), bf),
            dma((9,)),
            dma((3,)),
            dma((3,)),
            dma((count,)),
            dma((count,)),
            dma((count,)),
            dma((count,)),
            dma((count,)),
            dma((count,)),
        ],
        compiler_params=pltpu.CompilerParams(
            collective_id=1, has_side_effects=True, vmem_limit_bytes=VMEM_BYTES
        ),
    )(
        cell_out,
        w_all,
        tokens,
        ffn_gain[None, :],
        jnp.swapaxes(routes, 0, 1),
        jnp.swapaxes(route_weights, 0, 1),
        gate_t,
        up_t,
        down,
    )


def rms_scale(values_in, gain_vec):
    widened = values_in.astype(jnp.float32)
    return (
        widened * lax.rsqrt(jnp.mean(widened * widened, axis=-1, keepdims=True) + 1e-06) * gain_vec
    )


def memory_cell(
    query,
    key_row,
    value_row,
    outgate,
    input_pre,
    forget_pre,
    head_gain,
    state_matrix,
    state_norm,
    state_max,
):
    seq_rows, head_count = input_pre.shape
    head_size = query.shape[1] // head_count
    query_heads = query.astype(jnp.float32).reshape(seq_rows, head_count, head_size)
    key_heads = key_row.astype(jnp.float32).reshape(
        seq_rows, head_count, head_size
    ) * head_size ** (-0.5)
    value_heads = value_row.astype(jnp.float32).reshape(seq_rows, head_count, head_size)
    log_forget = jax.nn.log_sigmoid(forget_pre)
    new_max = jnp.maximum(log_forget + state_max, input_pre)
    keep_old = jnp.exp(log_forget + state_max - new_max)
    keep_new = jnp.exp(input_pre - new_max)
    new_matrix = (
        keep_old[:, :, None, None] * state_matrix
        + keep_new[:, :, None, None] * value_heads[:, :, :, None] * key_heads[:, :, None, :]
    )
    new_norm = keep_old[:, :, None] * state_norm + keep_new[:, :, None] * key_heads
    numerator = jnp.einsum(
        "bhvd,bhd->bhv", new_matrix, query_heads, precision=lax.Precision.HIGHEST
    )
    denominator = jnp.sum(new_norm * query_heads, axis=-1)
    cell_read = numerator / jnp.maximum(jnp.abs(denominator), jnp.exp(-new_max))[:, :, None]
    centered = cell_read - jnp.mean(cell_read, axis=-1, keepdims=True)
    variance = jnp.mean(centered * centered, axis=-1, keepdims=True)
    scaled_cell = (centered * lax.rsqrt(variance + 1e-06)).reshape(seq_rows, head_count * head_size)
    cell_out = (scaled_cell * head_gain * jax.nn.sigmoid(outgate.astype(jnp.float32))).astype(
        jnp.bfloat16
    )
    return (cell_out, new_matrix, new_norm, new_max)


def kernels_fit(tokens, w_query, w_igate, w_out, w_expert_gate, routes):
    ep_count = lax.axis_size("ep")
    rows, width = tokens.shape
    capacity = max(2, 2 * rows * routes.shape[1] // (w_expert_gate.shape[0] * ep_count))
    return (
        lax.axis_size("tp") == 2
        and ep_count % (2 * PLANE) == 0
        and w_query.shape[0] == LANES
        and w_query.shape[1] % LANES == 0
        and w_out.shape[1] % LANES == 0
        and width % (2 * LANES) == 0
        and rows % SLOT_TILE == 0
        and w_igate.shape[1] == 4
        and rows <= LANES
        and w_expert_gate.shape[0] == 1
        and capacity <= SLOT_TILE
    )


def body(
    tokens,
    mix_gain,
    w_query,
    w_key,
    w_value,
    w_outgate,
    w_igate,
    w_fgate,
    igate_bias,
    fgate_bias,
    head_gain,
    w_out,
    state_matrix,
    state_norm,
    state_max,
    ffn_gain,
    w_expert_gate,
    w_expert_up,
    w_expert_down,
    routes,
    route_weights,
):
    seq_rows, width = tokens.shape
    weight_list = (w_query, w_key, w_value, w_outgate, w_igate, w_fgate)
    if kernels_fit(tokens, w_query, w_igate, w_out, w_expert_gate, routes):
        proj, w_all = mixer_call(tokens, mix_gain, weight_list, w_out)
        cell_out, new_matrix, new_norm, new_max = cell_call(
            proj, igate_bias, fgate_bias, head_gain, state_matrix, state_norm, state_max
        )
        mixed = expert_call(
            cell_out,
            w_all,
            tokens,
            ffn_gain,
            routes,
            route_weights,
            w_expert_gate,
            w_expert_up,
            w_expert_down,
        )
        return (mixed, new_matrix, new_norm, new_max)
    normed = rms_scale(tokens, mix_gain).astype(jnp.bfloat16)
    spread = lax.all_to_all(normed, "ep", split_axis=1, concat_axis=0, tiled=True)
    joined = jnp.concatenate(weight_list, axis=1)
    summed = lax.psum_scatter(
        jnp.dot(spread, joined, preferred_element_type=jnp.float32),
        "ep",
        scatter_dimension=0,
        tiled=True,
    )
    bounds = [0]
    for weight in weight_list:
        bounds.append(bounds[-1] + weight.shape[1])
    projected = tuple(
        (summed[:, bounds[index] : bounds[index + 1]] for index in range(len(weight_list)))
    )
    query = projected[0].astype(jnp.bfloat16)
    key_row = projected[1].astype(jnp.bfloat16)
    value_row = projected[2].astype(jnp.bfloat16)
    outgate = projected[3].astype(jnp.bfloat16)
    input_pre = projected[4] + igate_bias
    forget_pre = projected[5] + fgate_bias
    cell_out, new_matrix, new_norm, new_max = memory_cell(
        query,
        key_row,
        value_row,
        outgate,
        input_pre,
        forget_pre,
        head_gain,
        state_matrix,
        state_norm,
        state_max,
    )
    partial_out = jnp.dot(
        cell_out,
        lax.all_gather(w_out, "ep", axis=1, tiled=True),
        preferred_element_type=jnp.float32,
    )
    attended = lax.psum(partial_out.astype(jnp.bfloat16), "tp").astype(jnp.float32)
    resid = (tokens.astype(jnp.float32) + attended).astype(jnp.bfloat16)
    normed_two = rms_scale(resid, ffn_gain).astype(jnp.bfloat16)
    ep_count = lax.axis_size("ep")
    local_experts = w_expert_gate.shape[0]
    expert_total = local_experts * ep_count
    top_count = routes.shape[1]
    capacity = max(2, 2 * seq_rows * top_count // expert_total)
    flat_routes = routes.reshape(-1)
    onehot = (flat_routes[:, None] == jnp.arange(expert_total, dtype=jnp.int32)[None, :]).astype(
        jnp.int32
    )
    earlier = jnp.cumsum(onehot, axis=0, dtype=jnp.int32) - onehot
    slots = jnp.sum(onehot * earlier, axis=1, dtype=jnp.int32)
    targets = flat_routes * capacity + slots
    dispatch = (
        targets[:, None] == jnp.arange(expert_total * capacity, dtype=jnp.int32)[None, :]
    ).astype(jnp.bfloat16)
    route_rows = jnp.repeat(normed_two, top_count, axis=0)
    outgoing = jnp.einsum(
        "rs,rd->sd", dispatch, route_rows, preferred_element_type=jnp.float32
    ).astype(jnp.bfloat16)
    outgoing = outgoing.reshape(expert_total, capacity, width)
    received = lax.all_to_all(outgoing, "ep", split_axis=0, concat_axis=0, tiled=True)
    slot_count = received.shape[1]
    regrouped = received.reshape(ep_count, local_experts, slot_count, width)
    gate_pre = jnp.einsum(
        "nxcd,xdf->nxcf", regrouped, w_expert_gate, preferred_element_type=jnp.float32
    )
    up_pre = jnp.einsum(
        "nxcd,xdf->nxcf", regrouped, w_expert_up, preferred_element_type=jnp.float32
    )
    hidden = (jax.nn.silu(gate_pre) * up_pre).astype(jnp.bfloat16)
    partial_down = jnp.einsum(
        "nxcf,xfd->nxcd", hidden, w_expert_down, preferred_element_type=jnp.float32
    )
    expert_sum = lax.psum(partial_down.astype(jnp.bfloat16), "tp")
    finished = expert_sum.reshape(ep_count * local_experts, slot_count, width)
    returned = lax.all_to_all(finished, "ep", split_axis=0, concat_axis=0, tiled=True)
    picked = jnp.dot(
        dispatch,
        returned.reshape(expert_total * capacity, width),
        preferred_element_type=jnp.float32,
    )
    weighted = jnp.sum(
        picked.reshape(seq_rows, top_count, width) * route_weights[:, :, None], axis=1
    )
    mixed = (resid.astype(jnp.float32) + weighted).astype(jnp.bfloat16)
    return (mixed, new_matrix, new_norm, new_max)


def solution(mesh):
    placed = (
        P("ep", None),
        P(),
        P("ep", "tp"),
        P("ep", "tp"),
        P("ep", "tp"),
        P("ep", "tp"),
        P("ep", "tp"),
        P("ep", "tp"),
        P("tp"),
        P("tp"),
        P("tp"),
        P("tp", "ep"),
        P("ep", "tp", None, None),
        P("ep", "tp", None),
        P("ep", "tp"),
        P(),
        P("ep", None, "tp"),
        P("ep", None, "tp"),
        P("ep", "tp", None),
        P("ep", None),
        P("ep", None),
    )
    return jax.shard_map(
        body,
        mesh=mesh,
        in_specs=placed,
        out_specs=(P("ep", None), P("ep", "tp", None, None), P("ep", "tp", None), P("ep", "tp")),
        check_vma=False,
    )
```

profile of v0, /device:TPU:29, one launch (start us, length us, event | category | flops | bytes accessed | tf_op | source)
XLA Modules:
  0.0 76.4 jit_solution(11527869408130246485)
XLA Ops:
  0.6 22.1 %shard_map.228 = (f32[32,1152]{1,0:T(8,128)}, bf16[4,4,256,128]{3,2,1,0:T(8,128)(2,1)}) custom-call(bf16[32,2048]{1,0:T(8,128)(2,1)} %tokens_hbm.3, f32[1,2048]{1,0:T(1,128)} %bitcast.21, bf16[128,256]{1,0:T(8,128)(2,1)} %wq_ref.1, bf16[128,256]{1,0:T(8,128)(2,1)} %wk_ref.1, bf16[128,256]{1,0:T(8,128)(2,1)} %wv_ref.1, bf16[128,256]{1,0:T(8,128)(2,1)} %wo_gate_ref.1, ...), custom_call_target="tpu_custom_call" | custom-call | tf_op jit(solution)/shard_map/pallas_call | solution.py:581
  22.7 9.9 %shard_map.229 = (bf16[32,256]{1,0:T(8,128)(2,1)}, f32[32,4,64,64]{3,2,1,0:T(8,128)}, f32[32,4,64]{2,1,0:T(4,128)}, f32[4,32]{1,0:T(4,128)}) custom-call(f32[32,1152]{1,0:T(8,128)} %get-tuple-element.10.proj_ref, f32[1,4]{1,0:T(1,128)} %bitcast.29, f32[1,4]{1,0:T(1,128)} %bitcast.30, f32[1,256]{1,0:T(1,128)} %bitcast.28, f32[32,4,64,64]{3,2,1,0:T(8,128)} %matrix_hbm.1, ...), custom_call_target="tpu_custom_call" | custom-call | tf_op jit(solution)/shard_map/pallas_call | solution.py:637
  32.6 42.2 %shard_map.230 = bf16[32,2048]{1,0:T(8,128)(2,1)} custom-call(bf16[32,256]{1,0:T(8,128)(2,1)} %get-tuple-element.11.cell_hbm, bf16[4,4,256,128]{3,2,1,0:T(8,128)(2,1)} %get-tuple-element.12.w_all_hbm, bf16[32,2048]{1,0:T(8,128)(2,1)} %tokens_hbm.3, f32[1,2048]{1,0:T(1,128)} %bitcast.22, s32[3,32]{1,0:T(4,128)} %bitcast.24, f32[3,32]{1,0:T(4,128)} %bitcast.25, ...), custom_call_target="tpu_custom_call" | custom-call | tf_op jit(solution)/shard_map/pallas_call | solution.py:692
  74.9 1.6 %copy.26 = bf16[32,2048]{1,0:T(8,128)(2,1)} copy(bf16[32,2048]{1,0:T(8,128)(2,1)} %shard_map.230) | data formatting | bytes 262144
where the time goes:
time: 76.7 us; the launch traced here: 76.4 us
  Pallas kernels  74.2 us (97%)
  local copies, waits for them, and re-layouts  1.57 us (2%)
    pallas_call x1, Pallas kernels, expert_call(): pl.pallas_call(functools.partial(expert_kernel, count), out_shape=jax.Sha...  42.2 us
    pallas_call x1, Pallas kernels, mixer_call(): pl.pallas_call(functools.partial(mixer_kernel, lines), out_shape=(jax.Sha...  22.1 us
    pallas_call x1, Pallas kernels, cell_call(): pl.pallas_call(cell_kernel, out_shape=(jax.ShapeDtypeStruct((rows, wide),...  9.89 us
    unnamed x1, local copies, waits for them, and re-layouts  1.57 us

commit v1 on v0

v1 whole, which is shorter than its diff:
```python
import functools

import jax
import jax.numpy as jnp
from jax import lax
from jax.experimental import pallas as pl
from jax.experimental.pallas import tpu as pltpu
from jax.sharding import PartitionSpec as P

MESH = pl.DeviceIdType.MESH
PLANE = 4
LANES = 128
SUB = 8
LAYER_BYTES = 40 * 1024 * 1024
UPDATE_BYTES = 12 * 1024 * 1024


def remote(src, dst, send_sem, recv_sem, target):
    return pltpu.make_async_remote_copy(
        src_ref=src,
        dst_ref=dst,
        send_sem=send_sem,
        recv_sem=recv_sem,
        device_id=target,
        device_id_type=MESH,
    )


def dot_t(left, right):
    return lax.dot_general(
        left, right, (((1,), (1,)), ((), ())), preferred_element_type=jnp.float32
    )


def fetch_all(pairs, sems):
    copies = []
    for index, (source, kept) in enumerate(pairs):
        copy = pltpu.make_async_copy(source, kept, sems.at[index])
        copy.start()
        copies.append(copy)
    return copies


def place(index, size):
    return pl.ds(pl.multiple_of(index * size, size), size)


def split_three(values):
    high = values.astype(jnp.bfloat16)
    rest = values - high.astype(jnp.float32)
    middle = rest.astype(jnp.bfloat16)
    return [high, middle, (rest - middle.astype(jnp.float32)).astype(jnp.bfloat16)]


def exact_dot(values, chosen):
    rows = values[0].shape[0]
    parts = [part for value in values for part in split_three(value)]
    product = jnp.dot(
        jnp.concatenate(parts, axis=0), chosen, preferred_element_type=jnp.float32
    )
    results = []
    for index in range(len(values)):
        start = 3 * index * rows
        pieces = [product[start + rows * part : start + rows * (part + 1)] for part in range(3)]
        results.append(pieces[0] + pieces[1] + pieces[2])
    return results


def ones_where(condition):
    return jnp.where(condition, 1.0, 0.0).astype(jnp.bfloat16)


def gather_rows(chosen, values):
    return jnp.dot(chosen, values, preferred_element_type=jnp.float32).astype(jnp.bfloat16)


def layer_kernel(
    count,
    tokens_hbm,
    mix_gain_hbm,
    wq_hbm,
    wk_hbm,
    wv_hbm,
    wg_hbm,
    igate_hbm,
    fgate_hbm,
    ibias_hbm,
    fbias_hbm,
    head_gain_hbm,
    w_out_hbm,
    matrix_hbm,
    norm_hbm,
    max_hbm,
    ffn_gain_hbm,
    w_gate_hbm,
    w_up_hbm,
    w_down_hbm,
    routes_hbm,
    route_weights_hbm,
    mixed_ref,
    left_ref,
    keys_ref,
    decay_ref,
    new_norm_ref,
    new_max_ref,
    tokens,
    mix_gain,
    igate,
    fgate,
    ibias,
    fbias,
    head_gain,
    matrix,
    state_norm,
    state_max,
    ffn_gain,
    w_gate,
    w_up,
    w_down,
    routes,
    route_weights,
    turned,
    gate_rows,
    gate_t,
    weights_a,
    weights_b,
    w_planes,
    normed,
    spread,
    partial_a,
    partial_b,
    outgoing_a,
    outgoing_b,
    arrived_a,
    arrived_b,
    packed,
    chosen_out,
    chosen_in,
    token_out,
    token_near,
    token_far,
    cell_mine,
    cell_theirs,
    cell_out,
    cell_near,
    cell_far,
    token_rows,
    reads,
    resid,
    row_values,
    down_send,
    down_recv,
    finished,
    returned,
    last_send,
    last_recv,
    local_sem,
    a_send,
    a_recv,
    b_send,
    b_recv,
    g_send,
    g_recv,
    x_send,
    x_recv,
    z_send,
    z_recv,
    pa_send,
    pa_recv,
    pb_send,
    pb_recv,
    o_send,
    o_recv,
    t_send,
    t_recv,
    k_send,
    k_recv,
    c_send,
    c_recv,
    f_send,
    f_recv,
    r_send,
    r_recv,
):
    bf, f32 = jnp.bfloat16, jnp.float32
    ep, tp = lax.axis_index("ep"), lax.axis_index("tp")
    lines = count // PLANE
    line, spot = ep // PLANE, ep % PLANE
    rows, width = tokens.shape
    half = width // 2
    depth = wq_hbm.shape[0]
    block = depth * PLANE
    heads = igate.shape[0]
    size = matrix.shape[3]
    wide = heads * size
    pair = 2 * wide
    area = count * SUB
    top = route_weights.shape[0]
    columns = w_out_hbm.shape[1]
    slab = lines * columns
    part_wide = slab // 2
    partner = (ep, 1 - tp)
    beside = spot + 1 - 2 * (spot % 2)
    across = lax.rem(spot + 2, PLANE)
    beside_peer = (line * PLANE + beside, tp)
    across_peer = (line * PLANE + across, tp)
    corner_peer = (line * PLANE + PLANE - 1 - spot, tp)
    my_half, other_half = place(tp, half), place(1 - tp, half)
    my_rows, other_rows = place(tp, wide), place(1 - tp, wide)
    own_rows = place(spot, depth)

    def line_peer(step):
        other = lax.rem(line + step, lines)
        return other, (other * PLANE + spot, tp)

    first_loads = fetch_all(
        (
            (wq_hbm, weights_a.at[own_rows, :wide]),
            (wk_hbm, weights_a.at[own_rows, wide:]),
            (igate_hbm, igate),
            (fgate_hbm, fgate),
            (wv_hbm, weights_b.at[own_rows, :wide]),
            (wg_hbm, weights_b.at[own_rows, wide:]),
            (tokens_hbm, tokens),
            (mix_gain_hbm, mix_gain),
            (w_out_hbm, w_planes.at[spot, my_rows, place(line, columns)]),
            (routes_hbm, routes),
            (route_weights_hbm, route_weights),
        ),
        local_sem,
    )
    barrier = pltpu.get_barrier_semaphore()
    for step in range(1, count):
        pl.semaphore_signal(
            barrier, inc=1, device_id=(lax.rem(ep + step, count), tp), device_id_type=MESH
        )
    pl.semaphore_signal(barrier, inc=1, device_id=partner, device_id_type=MESH)
    turned[...] = jnp.zeros_like(turned)
    gate_t[...] = jnp.zeros_like(gate_t)
    for copy in first_loads[:4]:
        copy.wait()
    turned[:heads, :] = igate[...].astype(f32)
    turned[heads : 2 * heads, :] = fgate[...].astype(f32)
    gate_rows[spot] = turned[: 2 * heads, :].astype(bf)
    pl.semaphore_wait(barrier, count)

    def plane_copies(buffer_view, send, recv):
        def make(owner, part, slot, target):
            view = buffer_view(owner, part)
            return remote(view, view, send.at[slot], recv.at[slot], target)

        return make

    def weight_view(buffer):
        def view(owner, part):
            tall = depth // 2
            return buffer.at[pl.ds(pl.multiple_of(owner * depth + part * tall, tall), tall)]

        return view

    def out_view(owner, part):
        return w_planes.at[owner, my_rows, part * part_wide : (part + 1) * part_wide]

    def open_plane(make):
        first = [
            make(spot, 0, 0, beside_peer),
            make(spot, 1, 2, across_peer),
            make(spot, 1, 1, beside_peer),
            make(spot, 0, 3, across_peer),
        ]
        for copy in first:
            copy.start()
        return first

    def relay_plane(make, first):
        first[0].wait_recv()
        ahead = make(beside, 0, 4, across_peer)
        ahead.start()
        first[1].wait_recv()
        aside = make(across, 1, 5, beside_peer)
        aside.start()
        return [ahead, aside]

    def close_plane(first, second):
        first[2].wait_recv()
        first[3].wait_recv()
        for copy in first:
            copy.wait_send()
        for copy in second:
            copy.wait()

    make_a = plane_copies(weight_view(weights_a), a_send, a_recv)
    make_b = plane_copies(weight_view(weights_b), b_send, b_recv)
    make_o = plane_copies(out_view, o_send, o_recv)
    a_first = open_plane(make_a)
    gate_copies = []
    for slot, target in enumerate((beside_peer, across_peer, corner_peer)):
        view = gate_rows.at[spot]
        copy = remote(view, view, g_send.at[slot], g_recv.at[slot], target)
        copy.start()
        gate_copies.append(copy)
    for copy in first_loads[4:9]:
        copy.wait()
    widened = tokens[...].astype(f32)
    scale = lax.rsqrt(jnp.mean(widened * widened, axis=-1, keepdims=True) + 1e-06)
    normed[...] = (widened * scale * mix_gain[...]).astype(bf)
    x_copies, z_copies = [], []
    for step in range(1, lines):
        other, target = line_peer(step)
        copy = remote(
            normed.at[:, place(other, block)],
            spread.at[line],
            x_send.at[step],
            x_recv.at[step],
            target,
        )
        copy.start()
        x_copies.append(copy)
    for step in range(1, lines):
        view = w_planes.at[spot, my_rows, place(line, columns)]
        copy = remote(view, view, z_send.at[step], z_recv.at[step], line_peer(step)[1])
        copy.start()
        z_copies.append(copy)
    spread[line] = normed[:, place(line, block)]
    for copy in first_loads[9:]:
        copy.wait()
    late_loads = fetch_all(
        (
            (matrix_hbm, matrix),
            (norm_hbm, state_norm),
            (max_hbm, state_max),
            (ibias_hbm, ibias),
            (fbias_hbm, fbias),
            (head_gain_hbm, head_gain),
            (ffn_gain_hbm, ffn_gain),
            (w_gate_hbm, w_gate),
            (w_up_hbm, w_up),
            (w_down_hbm, w_down),
        ),
        local_sem,
    )

    slot_row = lax.broadcasted_iota(jnp.int32, (area, rows), 0).astype(f32)
    expert = lax.broadcasted_iota(jnp.int32, (count, rows), 0).astype(f32)
    before = jnp.where(
        lax.broadcasted_iota(jnp.int32, (rows, rows), 0)
        < lax.broadcasted_iota(jnp.int32, (rows, rows), 1),
        1.0,
        0.0,
    )
    taken = jnp.zeros((count, 1), f32)
    sent = [jnp.zeros((area, rows), f32) for _ in range(3)]
    mixes = [jnp.zeros((area, rows), f32) for _ in range(3)]
    for k in range(top):
        named = routes[k : k + 1, :].astype(f32)
        match = jnp.where(expert == named, 1.0, 0.0)
        earlier = jnp.dot(match, before, preferred_element_type=f32) + taken
        taken = taken + jnp.sum(match, axis=1, keepdims=True)
        position = jnp.sum(match * earlier, axis=0, keepdims=True)
        low = jnp.where(position < SUB, named * SUB + position, -1000.0)
        high = jnp.where(position < SUB, -1000.0, named * SUB + position - SUB)
        for index, target in enumerate((low, high, high + SUB // 2)):
            hit = slot_row == target
            sent[index] += jnp.where(hit, 1.0, 0.0)
            mixes[index] += jnp.where(hit, route_weights[k : k + 1, :], 0.0)
    for index in range(3):
        chosen_out[index] = sent[index].astype(bf)
        coarse = mixes[index].astype(bf).astype(f32)
        joined = jnp.concatenate(
            [coarse, mixes[index] - coarse, jnp.zeros((area, area - 2 * rows), f32)], axis=1
        )
        chosen_in[index] = joined.T[: 2 * rows].astype(bf)

    def pack_rows(values, target):
        middle = values.shape[1] // 2
        target[:, :, : 2 * middle] = gather_rows(chosen_out[0], values).reshape(
            count, SUB, 2 * middle
        )
        extra = jnp.dot(chosen_out[1], values[:, :middle], preferred_element_type=f32)
        extra += jnp.dot(chosen_out[2], values[:, middle:], preferred_element_type=f32)
        target[:, :, 2 * middle :] = extra.astype(bf).reshape(count, SUB, middle)

    a_second = relay_plane(make_a, a_first)
    b_first = open_plane(make_b)
    pack_rows(tokens[:, my_half], token_out)
    late_loads[0].wait()

    def pack_matrix(start, stop):
        @pl.loop(start, stop)
        def _(index):
            item = 2 * index
            joined = jnp.concatenate(
                [matrix[item].reshape(wide, size), matrix[item + 1].reshape(wide, size)], axis=1
            )
            flipped = joined.T
            upper = flipped.astype(bf)
            packed[index, : 2 * size] = upper
            packed[index, 2 * size :] = (flipped - upper.astype(f32)).astype(bf)

    pack_matrix(0, rows // 4)
    for copy in gate_copies:
        copy.wait()
    for owner in range(PLANE):
        part = gate_rows[owner]
        gate_t[: 2 * heads, owner * depth : (owner + 1) * depth] = part
        gate_t[LANES // 2 : LANES // 2 + 2 * heads, owner * depth : (owner + 1) * depth] = part
    for copy in x_copies:
        copy.wait()
    close_plane(a_first, a_second)
    arranged = spread[...].reshape(lines * rows, block)
    product = jnp.dot(arranged, weights_a[...], preferred_element_type=f32)
    gates = dot_t(arranged, gate_t[...])
    coarse = gates.astype(bf).astype(f32)
    first = lax.broadcasted_iota(jnp.int32, gates.shape, 1) < LANES // 2
    picked = jnp.where(first, coarse, gates - coarse).astype(bf)
    outgoing_a[:, :, :pair] = product.astype(bf).reshape(lines, rows, pair)
    outgoing_a[:, :, pair:] = picked.reshape(lines, rows, LANES)
    partial_a[:, :, :pair] = product.reshape(lines, rows, pair)
    partial_a[:, :, pair:] = jnp.where(first, gates, 0.0).reshape(lines, rows, LANES)

    def send_partials(outgoing, arrived, send, recv):
        copies = []
        for step in range(1, lines):
            other, target = line_peer(step)
            copy = remote(
                outgoing.at[other], arrived.at[step], send.at[step], recv.at[step], target
            )
            copy.start()
            copies.append(copy)
        return copies

    pa_copies = send_partials(outgoing_a, arrived_a, pa_send, pa_recv)
    b_second = relay_plane(make_b, b_first)
    pack_matrix(rows // 4, rows // 2)
    for copy in late_loads[1:7]:
        copy.wait()

    chosen_head = ones_where(
        lax.broadcasted_iota(jnp.int32, (LANES, pair), 0) % (LANES // 2)
        == lax.broadcasted_iota(jnp.int32, (LANES, pair), 1) // size
    )
    same_head = ones_where(
        lax.broadcasted_iota(jnp.int32, (wide, wide), 0) // size
        == lax.broadcasted_iota(jnp.int32, (wide, wide), 1) // size
    )
    same_place = ones_where(
        lax.broadcasted_iota(jnp.int32, (wide, wide), 0) % size
        == lax.broadcasted_iota(jnp.int32, (wide, wide), 1) % size
    )
    turned[...] = jnp.zeros_like(turned)
    turned[:heads, :rows] = state_max[...]
    old_max_lane = turned[...].T[:rows]
    turned[...] = jnp.zeros_like(turned)
    turned[0:1, :heads] = ibias[...]
    turned[1:2, :heads] = fbias[...]
    ibias_lane, fbias_lane = turned[0:1, :], turned[1:2, :]
    biases = jnp.concatenate(
        [ibias_lane + pltpu.roll(fbias_lane, heads, 1), jnp.zeros((7, LANES), f32)], axis=0
    )
    old_max_wide, bias_wide = (
        exact_dot([old_max_lane], chosen_head)[0][:, :wide],
        exact_dot([biases], chosen_head)[0][:1],
    )
    old_norm = jnp.concatenate([state_norm[:, head, :] for head in range(heads)], axis=1)

    for copy in z_copies:
        copy.wait()
    close_plane(b_first, b_second)
    product = jnp.dot(arranged, weights_b[...], preferred_element_type=f32)
    outgoing_b[...] = product.astype(bf).reshape(lines, rows, pair)
    partial_b[...] = product.reshape(lines, rows, pair)
    pb_copies = send_partials(outgoing_b, arrived_b, pb_send, pb_recv)
    o_first = open_plane(make_o)

    def scatter(source, near, send, recv):
        copies = []
        for step in range(1, count):
            other = lax.rem(ep + step, count)
            copy = remote(
                source.at[other], near.at[ep], send.at[step], recv.at[step], (other, tp)
            )
            copy.start()
            copies.append(copy)
        near[ep] = source[ep]
        return copies

    token_copies = scatter(token_out, token_near, k_send, k_recv)

    total = partial_a[line]
    for step in range(1, lines):
        pa_copies[step - 1].wait()
        total = total + arrived_a[step].astype(f32)
    gates_lane = total[:, pair:]
    gates_wide = exact_dot([gates_lane], chosen_head)[0]

    def gate_math(input_pre, forget_pre, old_max):
        log_forget = jnp.minimum(forget_pre, 0.0) - jnp.log(1.0 + jnp.exp(-jnp.abs(forget_pre)))
        new_max = jnp.maximum(log_forget + old_max, input_pre)
        return new_max, jnp.exp(log_forget + old_max - new_max), jnp.exp(input_pre - new_max)

    new_max, keep_old, keep_new = gate_math(
        gates_wide[:, :wide] + bias_wide[:, :wide],
        gates_wide[:, wide:] + bias_wide[:, wide:],
        old_max_wide,
    )
    query = total[:, :wide].astype(bf).astype(f32)
    key = total[:, wide:pair].astype(bf).astype(f32) * size ** (-0.5)
    pack = 2 * heads
    row = lax.broadcasted_iota(jnp.int32, (rows, pack, wide), 1)
    head = lax.broadcasted_iota(jnp.int32, (rows, pack, wide), 2) // size
    only = row == head
    spread_query = jnp.where(only, jnp.broadcast_to(query[:, None, :], only.shape), 0.0)
    tiled = jnp.dot(
        spread_query.reshape(rows * pack, wide).astype(bf),
        same_place,
        preferred_element_type=f32,
    )
    asked_shape = (rows * pack, wide)
    parity = (lax.broadcasted_iota(jnp.int32, asked_shape, 0) // pack) % 2
    lane_parity = (lax.broadcasted_iota(jnp.int32, asked_shape, 1) // size) % 2
    asked = jnp.where(parity == lane_parity, tiled, 0.0).astype(bf)
    for index in range(rows // 2):
        span = slice(2 * pack * index, 2 * pack * (index + 1))
        reads[span, :] = jnp.dot(asked[span], packed[index], preferred_element_type=f32)
    read_old = jnp.sum(jnp.where(only, reads[...].reshape(rows, pack, wide), 0.0), axis=1)
    query_key, query_norm = exact_dot([query * key, query * old_norm], same_head)
    divisor = jnp.maximum(
        jnp.abs(keep_old * query_norm + keep_new * query_key), jnp.exp(-new_max)
    )
    o_second = relay_plane(make_o, o_first)
    late = partial_b[line]
    for step in range(1, lines):
        pb_copies[step - 1].wait()
        late = late + arrived_b[step].astype(f32)
    value = late[:, :wide].astype(bf).astype(f32)
    outgate = late[:, wide:].astype(bf).astype(f32)
    read = (keep_old * read_old + keep_new * query_key * value) / divisor
    centered = read - exact_dot([read], same_head)[0] * (1.0 / size)
    variance = exact_dot([centered * centered], same_head)[0] * (1.0 / size)
    cell = (
        centered * lax.rsqrt(variance + 1e-06) * head_gain[...] * jax.nn.sigmoid(outgate)
    ).astype(bf)
    cell_mine[...] = cell
    swap = remote(cell_mine, cell_theirs, t_send.at[0], t_recv.at[0], partner)
    swap.start()
    pack_rows(cell, cell_out)
    cell_copies = scatter(cell_out, cell_near, c_send, c_recv)

    for copy in token_copies:
        copy.wait()
    token_swap = remote(token_near, token_far, t_send.at[1], t_recv.at[1], partner)
    token_swap.start()
    close_plane(o_first, o_second)
    out_slab = w_planes.at[:, my_rows]
    out_swap = remote(out_slab, out_slab, t_send.at[2], t_recv.at[2], partner)
    out_swap.start()

    lane_gates = gates_lane + pltpu.roll(gates_lane, LANES // 2, 1)
    lane_max, lane_old, lane_new = gate_math(
        lane_gates + ibias_lane,
        pltpu.roll(lane_gates, LANES - heads, 1) + fbias_lane,
        old_max_lane,
    )
    turned[:rows, :] = lane_max
    new_max_ref[...] = turned[...].T[:heads, :rows]
    row_lane = lax.broadcasted_iota(jnp.int32, (rows, pack, LANES), 1)
    lane = lax.broadcasted_iota(jnp.int32, (rows, pack, LANES), 2)
    chosen = ((row_lane == lane) | (row_lane == lane + heads)) & (lane < heads)

    def per_head(values):
        wider = jnp.broadcast_to(values[:, None, :], (rows, pack, LANES))
        return jnp.sum(jnp.where(chosen, wider, 0.0), axis=-1, keepdims=True)

    old_scale, new_scale = per_head(lane_old), per_head(lane_new)
    decay_ref[...] = jnp.broadcast_to(old_scale, decay_ref.shape)
    same = only | (row == head + heads)
    spread_key = jnp.where(same, jnp.broadcast_to(key[:, None, :], same.shape), 0.0)
    key_rows = jnp.dot(
        spread_key.reshape(rows * pack, wide).astype(bf),
        same_place[:, :size],
        preferred_element_type=f32,
    ).reshape(rows, pack, size)
    keys_ref[...] = key_rows
    new_norm_ref[...] = (
        old_scale[:, :heads] * state_norm[...] + (new_scale * key_rows)[:, :heads]
    )
    scaled = jnp.where(same, jnp.broadcast_to(value[:, None, :], same.shape) * new_scale, 0.0)
    coarse = scaled.astype(bf).astype(f32)
    left_ref[...] = jnp.where(row < heads, coarse, scaled - coarse)

    swap.wait()
    token_swap.wait()
    out_swap.wait()
    home_columns = pl.ds(pl.multiple_of(tp * part_wide, part_wide), part_wide)
    for owner in range(PLANE):
        added = jnp.dot(
            cell_mine[...], w_planes[owner, my_rows, home_columns], preferred_element_type=f32
        ) + jnp.dot(
            cell_theirs[...], w_planes[owner, other_rows, home_columns], preferred_element_type=f32
        )
        for index in range(lines // 2):
            start = (index * PLANE + owner) * columns
            resid[:, start : start + columns] = added[:, index * columns : (index + 1) * columns]
    resid[...] = (tokens[:, my_half].astype(f32) + resid[...]).astype(bf).astype(f32)

    extra_rows = area // 2
    lift_row = lax.broadcasted_iota(jnp.int32, (extra_rows, area), 0)
    lift_column = lax.broadcasted_iota(jnp.int32, (extra_rows, area), 1)
    lift_place = (lift_row // (SUB // 2)) * SUB + lift_row % (SUB // 2)
    lift_low = ones_where(lift_column == lift_place)
    lift_high = ones_where(lift_column == lift_place + SUB // 2)

    def unpack_rows(source):
        middle = source.shape[2] // 3
        flat = source[:, :, : 2 * middle].reshape(area, 2 * middle)
        extra = source[:, :, 2 * middle :].reshape(area, middle)
        joined = jnp.concatenate(
            [gather_rows(lift_low, extra), gather_rows(lift_high, extra)], axis=1
        )
        return jnp.concatenate([flat, joined], axis=0)

    token_rows[:, my_half] = unpack_rows(token_near)
    token_rows[:, other_half] = unpack_rows(token_far)

    forwards = []
    for step in range(count):
        source = lax.rem(ep + count - step, count)
        if step > 0:
            cell_copies[step - 1].wait()
        copy = remote(
            cell_near.at[source],
            cell_far.at[source],
            f_send.at[step],
            f_recv.at[step],
            partner,
        )
        copy.start()
        forwards.append(copy)
    near_rows = unpack_rows(cell_near)
    for copy in forwards:
        copy.wait()
    far_rows = unpack_rows(cell_far)
    squares = jnp.zeros((near_rows.shape[0], columns), f32)
    for owner in range(PLANE):
        added = jnp.dot(
            near_rows, w_planes[owner, my_rows], preferred_element_type=f32
        ) + jnp.dot(far_rows, w_planes[owner, other_rows], preferred_element_type=f32)
        for index in range(lines):
            start = (index * PLANE + owner) * columns
            place_columns = slice(start, start + columns)
            summed = (
                token_rows[:, place_columns].astype(f32)
                + added[:, index * columns : (index + 1) * columns]
            ).astype(bf)
            row_values[:, place_columns] = summed
            widened = summed.astype(f32)
            squares += widened * widened
    scale = lax.rsqrt(jnp.sum(squares, axis=-1, keepdims=True) * (1.0 / width) + 1e-06)
    row_values[...] = (row_values[...].astype(f32) * scale * ffn_gain[...]).astype(bf)
    for copy in late_loads[7:]:
        copy.wait()
    gate_pre = dot_t(row_values[...], w_gate[...])
    up_pre = dot_t(row_values[...], w_up[...])
    hidden = (gate_pre * jax.nn.sigmoid(gate_pre) * up_pre).astype(bf)
    down_send[...] = jnp.dot(
        hidden, w_down[:, other_half], preferred_element_type=f32
    ).astype(bf)
    swap = remote(down_send, down_recv, t_send.at[3], t_recv.at[3], partner)
    swap.start()
    kept = jnp.dot(hidden, w_down[:, my_half], preferred_element_type=f32).astype(bf)
    swap.wait()
    done = (kept.astype(f32) + down_recv[...].astype(f32)).astype(bf)
    finished[:, :, :half] = done[:area].reshape(count, SUB, half)
    turn = (((0,), (0,)), ((), ()))
    folded = lax.dot_general(
        lift_low, done[area:, : half // 2], turn, preferred_element_type=f32
    ) + lax.dot_general(lift_high, done[area:, half // 2 :], turn, preferred_element_type=f32)
    finished[:, :, half:] = folded.astype(bf).reshape(count, SUB, half // 2)
    return_copies = scatter(finished, returned, r_send, r_recv)
    for copy in return_copies:
        copy.wait()
    back = returned[:, :, :half].reshape(area, half)
    back_extra = returned[:, :, half:].reshape(area, half // 2)

    def combine(index, values):
        both = jnp.dot(chosen_in[index], values, preferred_element_type=f32)
        return both[:rows] + both[rows:]

    weighted = combine(0, back) + jnp.concatenate(
        [combine(1, back_extra), combine(2, back_extra)], axis=1
    )
    last_send[...] = (resid[...] + weighted).astype(bf)
    swap = remote(last_send, last_recv, t_send.at[4], t_recv.at[4], partner)
    swap.start()
    mixed_ref[:, my_half] = last_send[...]
    swap.wait()
    mixed_ref[:, other_half] = last_recv[...]


def update_kernel(
    mixed_ref,
    left_ref,
    keys_ref,
    decay_ref,
    norm_ref,
    max_ref,
    matrix_hbm,
    mixed_out,
    new_matrix_ref,
    new_norm_out,
    new_max_out,
    matrix,
    in_sems,
    out_sems,
):
    rows, heads, size, _ = matrix.shape
    wide = heads * size
    chunk = 8
    chunks = rows // chunk
    loads = []
    for index in range(chunks):
        part = pl.ds(index * chunk, chunk)
        copy = pltpu.make_async_copy(matrix_hbm.at[part], matrix.at[part], in_sems.at[index])
        copy.start()
        loads.append(copy)
    mixed_out[...] = mixed_ref[...]
    new_norm_out[...] = norm_ref[...]
    new_max_out[...] = max_ref[...]
    stores = []
    for index in range(chunks):
        loads[index].wait()

        @pl.loop(0, chunk // 4)
        def _(group):
            for inner in range(4):
                item = index * chunk + group * 4 + inner
                outer = lax.dot_general(
                    left_ref[item].astype(jnp.bfloat16),
                    keys_ref[item].astype(jnp.bfloat16),
                    (((0,), (0,)), ((), ())),
                    preferred_element_type=jnp.float32,
                ).reshape(heads, size, size)
                scale = decay_ref[item][:heads][:, None, :]
                matrix[item] = scale * matrix[item] + outer

        part = pl.ds(index * chunk, chunk)
        copy = pltpu.make_async_copy(matrix.at[part], new_matrix_ref.at[part], out_sems.at[index])
        copy.start()
        stores.append(copy)
    for copy in stores:
        copy.wait()


def layer_call(
    tokens,
    mix_gain,
    weight_list,
    igate_bias,
    fgate_bias,
    head_gain,
    w_out,
    state_matrix,
    state_norm,
    state_max,
    ffn_gain,
    expert_weights,
    routes,
    route_weights,
):
    rows, width = tokens.shape
    w_query, w_key, w_value, w_outgate, w_igate, w_fgate = weight_list
    depth, wide = w_query.shape
    count = lax.axis_size("ep")
    lines = count // PLANE
    heads = w_igate.shape[1]
    size = state_matrix.shape[3]
    half, block, pair, area = width // 2, depth * PLANE, 2 * wide, count * SUB
    slots = area + area // 2
    gate_t = jnp.swapaxes(expert_weights[0][0], 0, 1)
    up_t = jnp.swapaxes(expert_weights[1][0], 0, 1)
    down = expert_weights[2][0]
    vmem = pl.BlockSpec(memory_space=pltpu.VMEM)
    far = pl.BlockSpec(memory_space=pltpu.HBM)
    anywhere = pl.BlockSpec(memory_space=pl.ANY)
    dma = pltpu.SemaphoreType.DMA
    bf, f32 = jnp.bfloat16, jnp.float32
    shape = jax.ShapeDtypeStruct
    tile = (count, SUB, half + half // 2)
    thin = (count, SUB, wide + wide // 2)
    made = (
        shape((rows, width), bf),
        shape((rows, 2 * heads, wide), f32),
        shape((rows, 2 * heads, size), f32),
        shape((rows, 2 * heads, size), f32),
        shape(state_norm.shape, f32),
        shape((heads, rows), f32),
    )
    results = pl.pallas_call(
        functools.partial(layer_kernel, count),
        out_shape=made,
        in_specs=[far] * 21,
        out_specs=(vmem,) * 6,
        scratch_shapes=[
            pltpu.VMEM((rows, width), bf),
            pltpu.VMEM((1, width), f32),
            pltpu.VMEM((heads, depth), bf),
            pltpu.VMEM((heads, depth), bf),
            pltpu.VMEM((1, heads), f32),
            pltpu.VMEM((1, heads), f32),
            pltpu.VMEM((1, wide), f32),
            pltpu.VMEM(state_matrix.shape, f32),
            pltpu.VMEM(state_norm.shape, f32),
            pltpu.VMEM((heads, rows), f32),
            pltpu.VMEM((1, width), f32),
            pltpu.VMEM(gate_t.shape, bf),
            pltpu.VMEM(up_t.shape, bf),
            pltpu.VMEM(down.shape, bf),
            pltpu.VMEM((routes.shape[1], rows), jnp.int32),
            pltpu.VMEM((routes.shape[1], rows), f32),
            pltpu.VMEM((LANES, LANES), f32),
            pltpu.VMEM((PLANE, 2 * heads, depth), bf),
            pltpu.VMEM((LANES, block), bf),
            pltpu.VMEM((block, pair), bf),
            pltpu.VMEM((block, pair), bf),
            pltpu.VMEM((PLANE, pair, lines * w_out.shape[1]), bf),
            pltpu.VMEM((rows, width), bf),
            pltpu.VMEM((lines, rows, block), bf),
            pltpu.VMEM((lines, rows, pair + LANES), f32),
            pltpu.VMEM((lines, rows, pair), f32),
            pltpu.VMEM((lines, rows, pair + LANES), bf),
            pltpu.VMEM((lines, rows, pair), bf),
            pltpu.VMEM((lines, rows, pair + LANES), bf),
            pltpu.VMEM((lines, rows, pair), bf),
            pltpu.VMEM((rows // 2, wide, wide), bf),
            pltpu.VMEM((3, area, rows), bf),
            pltpu.VMEM((3, 2 * rows, area), bf),
            pltpu.VMEM(tile, bf),
            pltpu.VMEM(tile, bf),
            pltpu.VMEM(tile, bf),
            pltpu.VMEM((rows, wide), bf),
            pltpu.VMEM((rows, wide), bf),
            pltpu.VMEM(thin, bf),
            pltpu.VMEM(thin, bf),
            pltpu.VMEM(thin, bf),
            pltpu.VMEM((slots, width), bf),
            pltpu.VMEM((rows * 2 * heads, wide), f32),
            pltpu.VMEM((rows, half), f32),
            pltpu.VMEM((slots, width), bf),
            pltpu.VMEM((slots, half), bf),
            pltpu.VMEM((slots, half), bf),
            pltpu.VMEM(tile, bf),
            pltpu.VMEM(tile, bf),
            pltpu.VMEM((rows, half), bf),
            pltpu.VMEM((rows, half), bf),
            dma((11,)),
            dma((6,)),
            dma((6,)),
            dma((6,)),
            dma((6,)),
            dma((3,)),
            dma((3,)),
            dma((lines,)),
            dma((lines,)),
            dma((lines,)),
            dma((lines,)),
            dma((lines,)),
            dma((lines,)),
            dma((lines,)),
            dma((lines,)),
            dma((6,)),
            dma((6,)),
            dma((5,)),
            dma((5,)),
            dma((count,)),
            dma((count,)),
            dma((count,)),
            dma((count,)),
            dma((count,)),
            dma((count,)),
            dma((count,)),
            dma((count,)),
        ],
        compiler_params=pltpu.CompilerParams(
            collective_id=0, has_side_effects=True, vmem_limit_bytes=LAYER_BYTES
        ),
    )(
        tokens,
        mix_gain[None, :],
        w_query,
        w_key,
        w_value,
        w_outgate,
        jnp.swapaxes(w_igate, 0, 1),
        jnp.swapaxes(w_fgate, 0, 1),
        igate_bias[None, :],
        fgate_bias[None, :],
        head_gain[None, :],
        w_out,
        state_matrix,
        state_norm,
        jnp.swapaxes(state_max, 0, 1),
        ffn_gain[None, :],
        gate_t,
        up_t,
        down,
        jnp.swapaxes(routes, 0, 1),
        jnp.swapaxes(route_weights, 0, 1),
    )
    mixed, new_matrix, new_norm, new_max = pl.pallas_call(
        update_kernel,
        out_shape=(made[0], shape(state_matrix.shape, f32), made[4], made[5]),
        in_specs=[vmem] * 6 + [anywhere],
        out_specs=(vmem, anywhere, vmem, vmem),
        scratch_shapes=[
            pltpu.VMEM(state_matrix.shape, f32),
            dma((rows // 8,)),
            dma((rows // 8,)),
        ],
        compiler_params=pltpu.CompilerParams(vmem_limit_bytes=UPDATE_BYTES),
    )(*results, state_matrix)
    return mixed, new_matrix, new_norm, jnp.swapaxes(new_max, 0, 1)


def rms_scale(values_in, gain_vec):
    widened = values_in.astype(jnp.float32)
    return (
        widened * lax.rsqrt(jnp.mean(widened * widened, axis=-1, keepdims=True) + 1e-06) * gain_vec
    )


def memory_cell(
    query,
    key_row,
    value_row,
    outgate,
    input_pre,
    forget_pre,
    head_gain,
    state_matrix,
    state_norm,
    state_max,
):
    seq_rows, head_count = input_pre.shape
    head_size = query.shape[1] // head_count
    query_heads = query.astype(jnp.float32).reshape(seq_rows, head_count, head_size)
    key_heads = key_row.astype(jnp.float32).reshape(
        seq_rows, head_count, head_size
    ) * head_size ** (-0.5)
    value_heads = value_row.astype(jnp.float32).reshape(seq_rows, head_count, head_size)
    log_forget = jax.nn.log_sigmoid(forget_pre)
    new_max = jnp.maximum(log_forget + state_max, input_pre)
    keep_old = jnp.exp(log_forget + state_max - new_max)
    keep_new = jnp.exp(input_pre - new_max)
    new_matrix = (
        keep_old[:, :, None, None] * state_matrix
        + keep_new[:, :, None, None] * value_heads[:, :, :, None] * key_heads[:, :, None, :]
    )
    new_norm = keep_old[:, :, None] * state_norm + keep_new[:, :, None] * key_heads
    numerator = jnp.einsum(
        "bhvd,bhd->bhv", new_matrix, query_heads, precision=lax.Precision.HIGHEST
    )
    denominator = jnp.sum(new_norm * query_heads, axis=-1)
    cell_read = numerator / jnp.maximum(jnp.abs(denominator), jnp.exp(-new_max))[:, :, None]
    centered = cell_read - jnp.mean(cell_read, axis=-1, keepdims=True)
    variance = jnp.mean(centered * centered, axis=-1, keepdims=True)
    scaled_cell = (centered * lax.rsqrt(variance + 1e-06)).reshape(seq_rows, head_count * head_size)
    cell_out = (scaled_cell * head_gain * jax.nn.sigmoid(outgate.astype(jnp.float32))).astype(
        jnp.bfloat16
    )
    return (cell_out, new_matrix, new_norm, new_max)


def kernels_fit(tokens, w_query, w_igate, w_out, w_expert_gate, routes):
    ep_count = lax.axis_size("ep")
    rows, width = tokens.shape
    capacity = max(2, 2 * rows * routes.shape[1] // (w_expert_gate.shape[0] * ep_count))
    return (
        lax.axis_size("tp") == 2
        and ep_count % (2 * PLANE) == 0
        and w_query.shape[0] == LANES
        and w_query.shape[1] % LANES == 0
        and w_out.shape[1] % LANES == 0
        and width % (2 * LANES) == 0
        and rows % 16 == 0
        and w_igate.shape[1] == 4
        and rows <= LANES
        and w_expert_gate.shape[0] == 1
        and capacity == SUB + SUB // 2
        and ep_count * SUB == LANES
        and w_query.shape[1] == 2 * LANES
    )


def body(
    tokens,
    mix_gain,
    w_query,
    w_key,
    w_value,
    w_outgate,
    w_igate,
    w_fgate,
    igate_bias,
    fgate_bias,
    head_gain,
    w_out,
    state_matrix,
    state_norm,
    state_max,
    ffn_gain,
    w_expert_gate,
    w_expert_up,
    w_expert_down,
    routes,
    route_weights,
):
    seq_rows, width = tokens.shape
    weight_list = (w_query, w_key, w_value, w_outgate, w_igate, w_fgate)
    if kernels_fit(tokens, w_query, w_igate, w_out, w_expert_gate, routes):
        mixed, new_matrix, new_norm, new_max = layer_call(
            tokens,
            mix_gain,
            weight_list,
            igate_bias,
            fgate_bias,
            head_gain,
            w_out,
            state_matrix,
            state_norm,
            state_max,
            ffn_gain,
            (w_expert_gate, w_expert_up, w_expert_down),
            routes,
            route_weights,
        )
        return (mixed, new_matrix, new_norm, new_max)
    normed = rms_scale(tokens, mix_gain).astype(jnp.bfloat16)
    spread = lax.all_to_all(normed, "ep", split_axis=1, concat_axis=0, tiled=True)
    joined = jnp.concatenate(weight_list, axis=1)
    summed = lax.psum_scatter(
        jnp.dot(spread, joined, preferred_element_type=jnp.float32),
        "ep",
        scatter_dimension=0,
        tiled=True,
    )
    bounds = [0]
    for weight in weight_list:
        bounds.append(bounds[-1] + weight.shape[1])
    projected = tuple(
        (summed[:, bounds[index] : bounds[index + 1]] for index in range(len(weight_list)))
    )
    query = projected[0].astype(jnp.bfloat16)
    key_row = projected[1].astype(jnp.bfloat16)
    value_row = projected[2].astype(jnp.bfloat16)
    outgate = projected[3].astype(jnp.bfloat16)
    input_pre = projected[4] + igate_bias
    forget_pre = projected[5] + fgate_bias
    cell_out, new_matrix, new_norm, new_max = memory_cell(
        query,
        key_row,
        value_row,
        outgate,
        input_pre,
        forget_pre,
        head_gain,
        state_matrix,
        state_norm,
        state_max,
    )
    partial_out = jnp.dot(
        cell_out,
        lax.all_gather(w_out, "ep", axis=1, tiled=True),
        preferred_element_type=jnp.float32,
    )
    attended = lax.psum(partial_out.astype(jnp.bfloat16), "tp").astype(jnp.float32)
    resid = (tokens.astype(jnp.float32) + attended).astype(jnp.bfloat16)
    normed_two = rms_scale(resid, ffn_gain).astype(jnp.bfloat16)
    ep_count = lax.axis_size("ep")
    local_experts = w_expert_gate.shape[0]
    expert_total = local_experts * ep_count
    top_count = routes.shape[1]
    capacity = max(2, 2 * seq_rows * top_count // expert_total)
    flat_routes = routes.reshape(-1)
    onehot = (flat_routes[:, None] == jnp.arange(expert_total, dtype=jnp.int32)[None, :]).astype(
        jnp.int32
    )
    earlier = jnp.cumsum(onehot, axis=0, dtype=jnp.int32) - onehot
    slots = jnp.sum(onehot * earlier, axis=1, dtype=jnp.int32)
    targets = flat_routes * capacity + slots
    dispatch = (
        targets[:, None] == jnp.arange(expert_total * capacity, dtype=jnp.int32)[None, :]
    ).astype(jnp.bfloat16)
    route_rows = jnp.repeat(normed_two, top_count, axis=0)
    outgoing = jnp.einsum(
        "rs,rd->sd", dispatch, route_rows, preferred_element_type=jnp.float32
    ).astype(jnp.bfloat16)
    outgoing = outgoing.reshape(expert_total, capacity, width)
    received = lax.all_to_all(outgoing, "ep", split_axis=0, concat_axis=0, tiled=True)
    slot_count = received.shape[1]
    regrouped = received.reshape(ep_count, local_experts, slot_count, width)
    gate_pre = jnp.einsum(
        "nxcd,xdf->nxcf", regrouped, w_expert_gate, preferred_element_type=jnp.float32
    )
    up_pre = jnp.einsum(
        "nxcd,xdf->nxcf", regrouped, w_expert_up, preferred_element_type=jnp.float32
    )
    hidden = (jax.nn.silu(gate_pre) * up_pre).astype(jnp.bfloat16)
    partial_down = jnp.einsum(
        "nxcf,xfd->nxcd", hidden, w_expert_down, preferred_element_type=jnp.float32
    )
    expert_sum = lax.psum(partial_down.astype(jnp.bfloat16), "tp")
    finished = expert_sum.reshape(ep_count * local_experts, slot_count, width)
    returned = lax.all_to_all(finished, "ep", split_axis=0, concat_axis=0, tiled=True)
    picked = jnp.dot(
        dispatch,
        returned.reshape(expert_total * capacity, width),
        preferred_element_type=jnp.float32,
    )
    weighted = jnp.sum(
        picked.reshape(seq_rows, top_count, width) * route_weights[:, :, None], axis=1
    )
    mixed = (resid.astype(jnp.float32) + weighted).astype(jnp.bfloat16)
    return (mixed, new_matrix, new_norm, new_max)


def solution(mesh):
    placed = (
        P("ep", None),
        P(),
        P("ep", "tp"),
        P("ep", "tp"),
        P("ep", "tp"),
        P("ep", "tp"),
        P("ep", "tp"),
        P("ep", "tp"),
        P("tp"),
        P("tp"),
        P("tp"),
        P("tp", "ep"),
        P("ep", "tp", None, None),
        P("ep", "tp", None),
        P("ep", "tp"),
        P(),
        P("ep", None, "tp"),
        P("ep", None, "tp"),
        P("ep", "tp", None),
        P("ep", None),
        P("ep", None),
    )
    return jax.shard_map(
        body,
        mesh=mesh,
        in_specs=placed,
        out_specs=(P("ep", None), P("ep", "tp", None, None), P("ep", "tp", None), P("ep", "tp")),
        check_vma=False,
    )
```

time: 76.7 us -> 79.7 us (1.039)
  the two profiles are of different devices: /device:TPU:29 before, /device:TPU:0 now
where the time goes in v1:
time: 79.7 us; the launch traced here: 78.4 us
  Pallas kernels  57.4 us (72%)
  local copies, waits for them, and re-layouts  20.3 us (25%)
    pallas_call x1, Pallas kernels, layer_call(): pl.pallas_call(functools.partial(layer_kernel, count), out_shape=made, in...  53.2 us
    unnamed x42, local copies, waits for them, and re-layouts  20.3 us
    pallas_call x1, Pallas kernels, layer_call(): pl.pallas_call(update_kernel, out_shape=(made[0], shape(state_matrix.shap...  4.16 us

profile of v1, /device:TPU:0, one launch (start us, length us, event | category | flops | bytes accessed | tf_op | source)
XLA Modules:
  0.0 78.4 jit_solution(17002896623126828864)
XLA Ops:
  0.6 0.0 copy-start
  0.6 2.2 %copy-done = f32[32,4,64,64]{3,2,1,0:T(8,128)S(1)} copy-done((f32[32,4,64,64]{3,2,1,0:T(8,128)S(1)}, f32[32,4,64,64]{3,2,1,0:T(8,128)}, u32[]{:S(2)}) %copy-start) | copy-done | bytes 2097176
  2.8 0.0 copy-start.1
  2.8 1.8 %copy-done.1 = bf16[1,2048,704]{1,2,0:T(8,128)(2,1)S(1)} copy-done((bf16[1,2048,704]{1,2,0:T(8,128)(2,1)S(1)}, bf16[1,2048,704]{1,2,0:T(8,128)(2,1)}, u32[]{:S(2)}) %copy-start.1) | copy-done | bytes 2883608
  4.6 0.0 copy-start.2
  4.6 1.8 %copy-done.2 = bf16[1,2048,704]{1,2,0:T(8,128)(2,1)S(1)} copy-done((bf16[1,2048,704]{1,2,0:T(8,128)(2,1)S(1)}, bf16[1,2048,704]{1,2,0:T(8,128)(2,1)}, u32[]{:S(2)}) %copy-start.2) | copy-done | bytes 2883608
  6.5 0.0 copy-start.3
  6.5 1.8 %copy-done.3 = bf16[1,704,2048]{2,1,0:T(8,128)(2,1)S(1)} copy-done((bf16[1,704,2048]{2,1,0:T(8,128)(2,1)S(1)}, bf16[1,704,2048]{2,1,0:T(8,128)(2,1)}, u32[]{:S(2)}) %copy-start.3) | copy-done | bytes 2883608
  8.3 0.0 copy-start.4
  8.3 0.9 %copy-done.4 = bf16[32,2048]{1,0:T(8,128)(2,1)S(1)} copy-done((bf16[32,2048]{1,0:T(8,128)(2,1)S(1)}, bf16[32,2048]{1,0:T(8,128)(2,1)}, u32[]{:S(2)}) %copy-start.4) | copy-done | bytes 131096
  9.2 0.0 copy-start.5
  9.2 0.8 %copy-done.5 = bf16[128,256]{1,0:T(8,128)(2,1)S(1)} copy-done((bf16[128,256]{1,0:T(8,128)(2,1)S(1)}, bf16[128,256]{1,0:T(8,128)(2,1)}, u32[]{:S(2)}) %copy-start.5) | copy-done | bytes 65560
  10.0 0.0 copy-start.6
  10.0 0.8 %copy-done.6 = bf16[128,256]{1,0:T(8,128)(2,1)S(1)} copy-done((bf16[128,256]{1,0:T(8,128)(2,1)S(1)}, bf16[128,256]{1,0:T(8,128)(2,1)}, u32[]{:S(2)}) %copy-start.6) | copy-done | bytes 65560
  10.9 0.0 copy-start.7
  10.9 0.8 %copy-done.7 = bf16[128,256]{1,0:T(8,128)(2,1)S(1)} copy-done((bf16[128,256]{1,0:T(8,128)(2,1)S(1)}, bf16[128,256]{1,0:T(8,128)(2,1)}, u32[]{:S(2)}) %copy-start.7) | copy-done | bytes 65560
  11.7 0.0 copy-start.8
  11.7 0.8 %copy-done.8 = bf16[128,256]{1,0:T(8,128)(2,1)S(1)} copy-done((bf16[128,256]{1,0:T(8,128)(2,1)S(1)}, bf16[128,256]{1,0:T(8,128)(2,1)}, u32[]{:S(2)}) %copy-start.8) | copy-done | bytes 65560
  12.5 0.0 copy-start.9
  12.5 0.8 %copy-done.9 = bf16[256,128]{1,0:T(8,128)(2,1)S(1)} copy-done((bf16[256,128]{1,0:T(8,128)(2,1)S(1)}, bf16[256,128]{1,0:T(8,128)(2,1)}, u32[]{:S(2)}) %copy-start.9) | copy-done | bytes 65560
  13.4 0.0 copy-start.10
  13.4 0.8 %copy-done.10 = f32[32,4,64]{2,1,0:T(4,128)S(1)} copy-done((f32[32,4,64]{2,1,0:T(4,128)S(1)}, f32[32,4,64]{2,1,0:T(4,128)}, u32[]{:S(2)}) %copy-start.10) | copy-done | bytes 32792
  14.2 0.0 copy-start.11
  14.2 0.7 copy-done.11
  14.9 0.0 copy-start.12
  14.9 0.7 copy-done.12
  15.6 0.0 copy-start.13
  15.6 0.7 copy-done.13
  16.3 0.0 copy-start.14
  16.3 0.7 copy-done.14
  17.0 0.0 copy-start.15
  17.0 0.7 copy-done.15
  17.7 0.0 copy-start.16
  17.7 0.7 copy-done.16
  18.3 0.0 copy-start.17
  18.3 0.7 copy-done.17
  19.0 0.0 copy-start.18
  19.0 0.7 copy-done.18
  19.7 0.0 copy-start.19
  19.7 0.7 copy-done.19
  20.4 0.0 copy-start.20
  20.4 0.7 copy-done.20
  21.0 53.2 %shard_map.228 = (bf16[32,2048]{1,0:T(8,128)(2,1)S(1)}, f32[32,8,256]{2,1,0:T(8,128)S(1)}, f32[32,8,64]{2,1,0:T(8,128)S(1)}, f32[32,8,64]{2,1,0:T(8,128)S(1)}, f...) custom-call(bf16[32,2048]{1,0:T(8,128)(2,1)S(1)} %copy-done.4, f32[1,2048]{1,0:T(1,128)S(1)} %bitcast.21, ...), custom_call_target="tpu_custom_call" | custom-call | tf_op jit(solution)/shard_map/pallas_call | solution.py:798
  74.2 4.2 %shard_map.229 = (bf16[32,2048]{1,0:T(8,128)(2,1)}, f32[32,4,64,64]{3,2,1,0:T(8,128)}, f32[32,4,64]{2,1,0:T(4,128)}, f32[4,32]{1,0:T(4,128)}) custom-call(bf16[32,2048]{1,0:T(8,128)(2,1)S(1)} %get-tuple-element.14.mixed_ref, f32[32,8,256]{2,1,0:T(8,128)S(1)} %get-tuple-element.15.left_ref, f32[32,8,64]{2,1,0:T(8,128)S(1)} %get-tuple-element.16.keys_ref, ...), custom_call_target="tpu_custom_call" | custom-call | tf_op jit(solution)/shard_map/pallas_call | solution.py:909
Async XLA Ops:
  0.6 2.2 %copy-start = (f32[32,4,64,64]{3,2,1,0:T(8,128)S(1)}, f32[32,4,64,64]{3,2,1,0:T(8,128)}, u32[]{:S(2)}) copy-start(f32[32,4,64,64]{3,2,1,0:T(8,128)} %matrix_hbm.3) | copy-start | bytes 6291460
  2.8 1.8 %copy-start.1 = (bf16[1,2048,704]{1,2,0:T(8,128)(2,1)S(1)}, bf16[1,2048,704]{1,2,0:T(8,128)(2,1)}, u32[]{:S(2)}) copy-start(bf16[1,2048,704]{1,2,0:T(8,128)(2,1)} %param.37) | copy-start | bytes 8650756
  4.6 1.8 %copy-start.2 = (bf16[1,2048,704]{1,2,0:T(8,128)(2,1)S(1)}, bf16[1,2048,704]{1,2,0:T(8,128)(2,1)}, u32[]{:S(2)}) copy-start(bf16[1,2048,704]{1,2,0:T(8,128)(2,1)} %param.38) | copy-start | bytes 8650756
  6.5 1.8 %copy-start.3 = (bf16[1,704,2048]{2,1,0:T(8,128)(2,1)S(1)}, bf16[1,704,2048]{2,1,0:T(8,128)(2,1)}, u32[]{:S(2)}) copy-start(bf16[1,704,2048]{2,1,0:T(8,128)(2,1)} %param.39) | copy-start | bytes 8650756
  8.3 0.9 %copy-start.4 = (bf16[32,2048]{1,0:T(8,128)(2,1)S(1)}, bf16[32,2048]{1,0:T(8,128)(2,1)}, u32[]{:S(2)}) copy-start(bf16[32,2048]{1,0:T(8,128)(2,1)} %tokens_hbm.1) | copy-start | bytes 393220
  9.2 0.8 %copy-start.5 = (bf16[128,256]{1,0:T(8,128)(2,1)S(1)}, bf16[128,256]{1,0:T(8,128)(2,1)}, u32[]{:S(2)}) copy-start(bf16[128,256]{1,0:T(8,128)(2,1)} %wq_hbm.1) | copy-start | bytes 196612
  10.0 0.8 %copy-start.6 = (bf16[128,256]{1,0:T(8,128)(2,1)S(1)}, bf16[128,256]{1,0:T(8,128)(2,1)}, u32[]{:S(2)}) copy-start(bf16[128,256]{1,0:T(8,128)(2,1)} %wk_hbm.1) | copy-start | bytes 196612
  10.9 0.8 %copy-start.7 = (bf16[128,256]{1,0:T(8,128)(2,1)S(1)}, bf16[128,256]{1,0:T(8,128)(2,1)}, u32[]{:S(2)}) copy-start(bf16[128,256]{1,0:T(8,128)(2,1)} %wv_hbm.1) | copy-start | bytes 196612
  11.7 0.8 %copy-start.8 = (bf16[128,256]{1,0:T(8,128)(2,1)S(1)}, bf16[128,256]{1,0:T(8,128)(2,1)}, u32[]{:S(2)}) copy-start(bf16[128,256]{1,0:T(8,128)(2,1)} %wg_hbm.1) | copy-start | bytes 196612
  12.5 0.8 %copy-start.9 = (bf16[256,128]{1,0:T(8,128)(2,1)S(1)}, bf16[256,128]{1,0:T(8,128)(2,1)}, u32[]{:S(2)}) copy-start(bf16[256,128]{1,0:T(8,128)(2,1)} %w_out_hbm.1) | copy-start | bytes 196612
  13.4 0.8 %copy-start.10 = (f32[32,4,64]{2,1,0:T(4,128)S(1)}, f32[32,4,64]{2,1,0:T(4,128)}, u32[]{:S(2)}) copy-start(f32[32,4,64]{2,1,0:T(4,128)} %norm_hbm.1) | copy-start | bytes 98308
  14.2 0.7 copy-start.11
  14.9 0.7 copy-start.12
  15.6 0.7 copy-start.13
  16.3 0.7 copy-start.14
  17.0 0.7 copy-start.15
  17.7 0.7 copy-start.16
  18.3 0.7 copy-start.17
  19.0 0.7 copy-start.18
  19.7 0.7 copy-start.19
  20.4 0.7 copy-start.20

commit v2 on v1

--- a/solution.py
+++ b/solution.py
@@ -795,6 +795,29 @@
         shape(state_norm.shape, f32),
         shape((heads, rows), f32),
     )
+    operands = (
+        tokens,
+        mix_gain[None, :],
+        w_query,
+        w_key,
+        w_value,
+        w_outgate,
+        jnp.swapaxes(w_igate, 0, 1),
+        jnp.swapaxes(w_fgate, 0, 1),
+        igate_bias[None, :],
+        fgate_bias[None, :],
+        head_gain[None, :],
+        w_out,
+        state_matrix,
+        state_norm,
+        jnp.swapaxes(state_max, 0, 1),
+        ffn_gain[None, :],
+        gate_t,
+        up_t,
+        down,
+        jnp.swapaxes(routes, 0, 1),
+        jnp.swapaxes(route_weights, 0, 1),
+    )
     results = pl.pallas_call(
         functools.partial(layer_kernel, count),
         out_shape=made,
@@ -883,29 +906,7 @@
         compiler_params=pltpu.CompilerParams(
             collective_id=0, has_side_effects=True, vmem_limit_bytes=LAYER_BYTES
         ),
-    )(
-        tokens,
-        mix_gain[None, :],
-        w_query,
-        w_key,
-        w_value,
-        w_outgate,
-        jnp.swapaxes(w_igate, 0, 1),
-        jnp.swapaxes(w_fgate, 0, 1),
-        igate_bias[None, :],
-        fgate_bias[None, :],
-        head_gain[None, :],
-        w_out,
-        state_matrix,
-        state_norm,
-        jnp.swapaxes(state_max, 0, 1),
-        ffn_gain[None, :],
-        gate_t,
-        up_t,
-        down,
-        jnp.swapaxes(routes, 0, 1),
-        jnp.swapaxes(route_weights, 0, 1),
-    )
+    )(*[pltpu.with_memory_space_constraint(operand, pltpu.HBM) for operand in operands])
     mixed, new_matrix, new_norm, new_max = pl.pallas_call(
         update_kernel,
         out_shape=(made[0], shape(state_matrix.shape, f32), made[4], made[5]),

time: 79.7 us -> 58.5 us (0.73)
  local copies, waits for them, and re-layouts: 20.3 us -> 0.01 us
    unnamed x42 -> x2, local copies, waits for them, and re-layouts: 20.3 us -> 0.01 us
where the time goes in v2:
time: 58.5 us; the launch traced here: 57.8 us
  Pallas kernels  57.2 us (98%)
  between operations  0.66 us (1%)
    pallas_call x1, Pallas kernels, layer_call(): pl.pallas_call(functools.partial(layer_kernel, count), out_shape=made, in...  53 us
    pallas_call x1, Pallas kernels, layer_call(): pl.pallas_call(update_kernel, out_shape=(made[0], shape(state_matrix.shap...  4.16 us

profile of v2, /device:TPU:0, one launch (start us, length us, event | category | flops | bytes accessed | tf_op | source)
XLA Modules:
  0.0 57.8 jit_solution(17985408994110283956)
XLA Ops:
  0.6 0.0 copy-start
  0.7 53.0 %shard_map.228 = (bf16[32,2048]{1,0:T(8,128)(2,1)S(1)}, f32[32,8,256]{2,1,0:T(8,128)S(1)}, f32[32,8,64]{2,1,0:T(8,128)S(1)}, f32[32,8,64]{2,1,0:T(8,128)S(1)}, f...) custom-call(bf16[32,2048]{1,0:T(8,128)(2,1)} %tokens_hbm.1, f32[1,2048]{1,0:T(1,128)} %bitcast.21, bf16[128,256]{1,0:T(8,128)(2,1)} %wq_hbm.1, ...), custom_call_target="tpu_custom_call" | custom-call | tf_op jit(solution)/shard_map/pallas_call | solution.py:821
  53.7 0.0 copy-done
  53.7 4.2 %shard_map.229 = (bf16[32,2048]{1,0:T(8,128)(2,1)}, f32[32,4,64,64]{3,2,1,0:T(8,128)}, f32[32,4,64]{2,1,0:T(4,128)}, f32[4,32]{1,0:T(4,128)}) custom-call(bf16[32,2048]{1,0:T(8,128)(2,1)S(1)} %get-tuple-element.14.mixed_ref, f32[32,8,256]{2,1,0:T(8,128)S(1)} %get-tuple-element.15.left_ref, f32[32,8,64]{2,1,0:T(8,128)S(1)} %get-tuple-element.16.keys_ref, ...), custom_call_target="tpu_custom_call" | custom-call | tf_op jit(solution)/shard_map/pallas_call | solution.py:910
Async XLA Ops:
  0.6 53.0 %copy-start = (f32[32,4,64,64]{3,2,1,0:T(8,128)S(1)}, f32[32,4,64,64]{3,2,1,0:T(8,128)}, u32[]{:S(2)}) copy-start(f32[32,4,64,64]{3,2,1,0:T(8,128)} %matrix_hbm.3) | copy-start | bytes 6291460

commit v3 on v2

--- a/solution.py
+++ b/solution.py
@@ -12,7 +12,7 @@
 LANES = 128
 SUB = 8
 LAYER_BYTES = 40 * 1024 * 1024
-UPDATE_BYTES = 12 * 1024 * 1024
+STORE_BYTES = 8 * 1024 * 1024
 
 
 def remote(src, dst, send_sem, recv_sem, target):
@@ -98,9 +98,7 @@
     routes_hbm,
     route_weights_hbm,
     mixed_ref,
-    left_ref,
-    keys_ref,
-    decay_ref,
+    new_matrix_ref,
     new_norm_ref,
     new_max_ref,
     tokens,
@@ -146,6 +144,9 @@
     cell_far,
     token_rows,
     reads,
+    left,
+    keys,
+    decay,
     resid,
     row_values,
     down_send,
@@ -163,6 +164,8 @@
     g_recv,
     x_send,
     x_recv,
+    y_send,
+    y_recv,
     z_send,
     z_recv,
     pa_send,
@@ -175,12 +178,17 @@
     t_recv,
     k_send,
     k_recv,
+    kf_send,
+    kf_recv,
     c_send,
     c_recv,
     f_send,
     f_recv,
+    w_send,
+    w_recv,
     r_send,
     r_recv,
+    ready,
 ):
     bf, f32 = jnp.bfloat16, jnp.float32
     ep, tp = lax.axis_index("ep"), lax.axis_index("tp")
@@ -230,11 +238,10 @@
         local_sem,
     )
     barrier = pltpu.get_barrier_semaphore()
-    for step in range(1, count):
-        pl.semaphore_signal(
-            barrier, inc=1, device_id=(lax.rem(ep + step, count), tp), device_id_type=MESH
-        )
-    pl.semaphore_signal(barrier, inc=1, device_id=partner, device_id_type=MESH)
+    greeted = [beside_peer, across_peer, corner_peer, partner]
+    greeted += [line_peer(step)[1] for step in range(1, lines)]
+    for target in greeted:
+        pl.semaphore_signal(barrier, inc=1, device_id=target, device_id_type=MESH)
     turned[...] = jnp.zeros_like(turned)
     gate_t[...] = jnp.zeros_like(gate_t)
     for copy in first_loads[:4]:
@@ -242,7 +249,9 @@
     turned[:heads, :] = igate[...].astype(f32)
     turned[heads : 2 * heads, :] = fgate[...].astype(f32)
     gate_rows[spot] = turned[: 2 * heads, :].astype(bf)
-    pl.semaphore_wait(barrier, count)
+    pl.semaphore_wait(barrier, len(greeted))
+    for step in range(1, lines):
+        pl.semaphore_signal(ready, inc=1, device_id=line_peer(step)[1], device_id_type=MESH)
 
     def plane_copies(buffer_view, send, recv):
         def make(owner, part, slot, target):
@@ -305,11 +314,13 @@
     scale = lax.rsqrt(jnp.mean(widened * widened, axis=-1, keepdims=True) + 1e-06)
     normed[...] = (widened * scale * mix_gain[...]).astype(bf)
     x_copies, z_copies = [], []
+    narrow = block // 2
+    my_part = place(tp, narrow)
     for step in range(1, lines):
         other, target = line_peer(step)
         copy = remote(
-            normed.at[:, place(other, block)],
-            spread.at[line],
+            normed.at[:, place(other * 2 + tp, narrow)],
+            spread.at[line, :, my_part],
             x_send.at[step],
             x_recv.at[step],
             target,
@@ -397,6 +408,13 @@
             packed[index, : 2 * size] = upper
             packed[index, 2 * size :] = (flipped - upper.astype(f32)).astype(bf)
 
+    y_copies = []
+    for step in range(1, lines):
+        x_copies[step - 1].wait()
+        view = spread.at[lax.rem(line + lines - step, lines), :, my_part]
+        copy = remote(view, view, y_send.at[step], y_recv.at[step], partner)
+        copy.start()
+        y_copies.append(copy)
     pack_matrix(0, rows // 4)
     for copy in gate_copies:
         copy.wait()
@@ -404,7 +422,7 @@
         part = gate_rows[owner]
         gate_t[: 2 * heads, owner * depth : (owner + 1) * depth] = part
         gate_t[LANES // 2 : LANES // 2 + 2 * heads, owner * depth : (owner + 1) * depth] = part
-    for copy in x_copies:
+    for copy in y_copies:
         copy.wait()
     close_plane(a_first, a_second)
     arranged = spread[...].reshape(lines * rows, block)
@@ -431,6 +449,18 @@
 
     pa_copies = send_partials(outgoing_a, arrived_a, pa_send, pa_recv)
     b_second = relay_plane(make_b, b_first)
+    for copy in z_copies:
+        copy.wait()
+    o_first = open_plane(make_o)
+    slabs = []
+
+    def pass_slab(view):
+        slot = len(slabs)
+        copy = remote(view, view, w_send.at[slot], w_recv.at[slot], partner)
+        copy.start()
+        slabs.append(copy)
+
+    pass_slab(w_planes.at[spot, my_rows])
     pack_matrix(rows // 4, rows // 2)
     for copy in late_loads[1:7]:
         copy.wait()
@@ -463,27 +493,41 @@
     )
     old_norm = jnp.concatenate([state_norm[:, head, :] for head in range(heads)], axis=1)
 
-    for copy in z_copies:
-        copy.wait()
     close_plane(b_first, b_second)
     product = jnp.dot(arranged, weights_b[...], preferred_element_type=f32)
     outgoing_b[...] = product.astype(bf).reshape(lines, rows, pair)
     partial_b[...] = product.reshape(lines, rows, pair)
     pb_copies = send_partials(outgoing_b, arrived_b, pb_send, pb_recv)
-    o_first = open_plane(make_o)
 
     def scatter(source, near, send, recv):
+        groups = {}
+        for hop in [lines // 2] + [n for n in range(1, lines) if n != lines // 2] + [0]:
+            groups[hop] = []
+            for turn in range(PLANE):
+                if hop == 0 and turn == 0:
+                    continue
+                other = lax.rem(line + hop, lines) * PLANE + lax.rem(spot + turn, PLANE)
+                slot = hop * PLANE + turn
+                copy = remote(
+                    source.at[other], near.at[ep], send.at[slot], recv.at[slot], (other, tp)
+                )
+                copy.start()
+                groups[hop].append(copy)
+        near[ep] = source[ep]
+        return groups
+
+    def forward(groups, near, far, send, recv):
         copies = []
-        for step in range(1, count):
-            other = lax.rem(ep + step, count)
-            copy = remote(
-                source.at[other], near.at[ep], send.at[step], recv.at[step], (other, tp)
-            )
+        for hop in range(lines):
+            for copy in groups[hop]:
+                copy.wait()
+            span = place(lax.rem(line + lines - hop, lines), PLANE)
+            copy = remote(near.at[span], far.at[span], send.at[hop], recv.at[hop], partner)
             copy.start()
             copies.append(copy)
-        near[ep] = source[ep]
         return copies
 
+    pl.semaphore_wait(ready, lines - 1)
     token_copies = scatter(token_out, token_near, k_send, k_recv)
 
     total = partial_a[line]
@@ -528,6 +572,8 @@
         jnp.abs(keep_old * query_norm + keep_new * query_key), jnp.exp(-new_max)
     )
     o_second = relay_plane(make_o, o_first)
+    pass_slab(out_view(beside, 0))
+    pass_slab(out_view(across, 1))
     late = partial_b[line]
     for step in range(1, lines):
         pb_copies[step - 1].wait()
@@ -546,14 +592,10 @@
     pack_rows(cell, cell_out)
     cell_copies = scatter(cell_out, cell_near, c_send, c_recv)
 
-    for copy in token_copies:
-        copy.wait()
-    token_swap = remote(token_near, token_far, t_send.at[1], t_recv.at[1], partner)
-    token_swap.start()
-    close_plane(o_first, o_second)
-    out_slab = w_planes.at[:, my_rows]
-    out_swap = remote(out_slab, out_slab, t_send.at[2], t_recv.at[2], partner)
-    out_swap.start()
+    o_first[2].wait_recv()
+    pass_slab(out_view(beside, 1))
+    o_first[3].wait_recv()
+    pass_slab(out_view(across, 0))
 
     lane_gates = gates_lane + pltpu.roll(gates_lane, LANES // 2, 1)
     lane_max, lane_old, lane_new = gate_math(
@@ -572,7 +614,7 @@
         return jnp.sum(jnp.where(chosen, wider, 0.0), axis=-1, keepdims=True)
 
     old_scale, new_scale = per_head(lane_old), per_head(lane_new)
-    decay_ref[...] = jnp.broadcast_to(old_scale, decay_ref.shape)
+    decay[...] = jnp.broadcast_to(old_scale, decay.shape)
     same = only | (row == head + heads)
     spread_key = jnp.where(same, jnp.broadcast_to(key[:, None, :], same.shape), 0.0)
     key_rows = jnp.dot(
@@ -580,28 +622,19 @@
         same_place[:, :size],
         preferred_element_type=f32,
     ).reshape(rows, pack, size)
-    keys_ref[...] = key_rows
+    keys[...] = key_rows
     new_norm_ref[...] = (
         old_scale[:, :heads] * state_norm[...] + (new_scale * key_rows)[:, :heads]
     )
     scaled = jnp.where(same, jnp.broadcast_to(value[:, None, :], same.shape) * new_scale, 0.0)
     coarse = scaled.astype(bf).astype(f32)
-    left_ref[...] = jnp.where(row < heads, coarse, scaled - coarse)
-
-    swap.wait()
-    token_swap.wait()
-    out_swap.wait()
-    home_columns = pl.ds(pl.multiple_of(tp * part_wide, part_wide), part_wide)
-    for owner in range(PLANE):
-        added = jnp.dot(
-            cell_mine[...], w_planes[owner, my_rows, home_columns], preferred_element_type=f32
-        ) + jnp.dot(
-            cell_theirs[...], w_planes[owner, other_rows, home_columns], preferred_element_type=f32
-        )
-        for index in range(lines // 2):
-            start = (index * PLANE + owner) * columns
-            resid[:, start : start + columns] = added[:, index * columns : (index + 1) * columns]
-    resid[...] = (tokens[:, my_half].astype(f32) + resid[...]).astype(bf).astype(f32)
+    left[...] = jnp.where(row < heads, coarse, scaled - coarse)
+
+    corner = PLANE - 1 - spot
+    token_forwards = forward(token_copies, token_near, token_far, kf_send, kf_recv)
+    for part in range(2):
+        o_second[part].wait_recv()
+        pass_slab(out_view(corner, part))
 
     extra_rows = area // 2
     lift_row = lax.broadcasted_iota(jnp.int32, (extra_rows, area), 0)
@@ -620,31 +653,28 @@
         return jnp.concatenate([flat, joined], axis=0)
 
     token_rows[:, my_half] = unpack_rows(token_near)
+    for copy in token_forwards:
+        copy.wait()
     token_rows[:, other_half] = unpack_rows(token_far)
 
-    forwards = []
-    for step in range(count):
-        source = lax.rem(ep + count - step, count)
-        if step > 0:
-            cell_copies[step - 1].wait()
-        copy = remote(
-            cell_near.at[source],
-            cell_far.at[source],
-            f_send.at[step],
-            f_recv.at[step],
-            partner,
-        )
-        copy.start()
-        forwards.append(copy)
+    forwards = forward(cell_copies, cell_near, cell_far, f_send, f_recv)
     near_rows = unpack_rows(cell_near)
+    for copy in o_first + o_second:
+        copy.wait_send()
+    near_parts = [
+        jnp.dot(near_rows, w_planes[owner, my_rows], preferred_element_type=f32)
+        for owner in range(PLANE)
+    ]
+    for copy in slabs:
+        copy.wait()
     for copy in forwards:
         copy.wait()
     far_rows = unpack_rows(cell_far)
     squares = jnp.zeros((near_rows.shape[0], columns), f32)
     for owner in range(PLANE):
-        added = jnp.dot(
-            near_rows, w_planes[owner, my_rows], preferred_element_type=f32
-        ) + jnp.dot(far_rows, w_planes[owner, other_rows], preferred_element_type=f32)
+        added = near_parts[owner] + jnp.dot(
+            far_rows, w_planes[owner, other_rows], preferred_element_type=f32
+        )
         for index in range(lines):
             start = (index * PLANE + owner) * columns
             place_columns = slice(start, start + columns)
@@ -662,92 +692,109 @@
     gate_pre = dot_t(row_values[...], w_gate[...])
     up_pre = dot_t(row_values[...], w_up[...])
     hidden = (gate_pre * jax.nn.sigmoid(gate_pre) * up_pre).astype(bf)
-    down_send[...] = jnp.dot(
-        hidden, w_down[:, other_half], preferred_element_type=f32
-    ).astype(bf)
-    swap = remote(down_send, down_recv, t_send.at[3], t_recv.at[3], partner)
-    swap.start()
-    kept = jnp.dot(hidden, w_down[:, my_half], preferred_element_type=f32).astype(bf)
+    quarter = half // 2
+    swaps, kept = [], []
+    for part in range(2):
+        theirs = w_down[:, place((1 - tp) * 2 + part, quarter)]
+        down_send[part] = jnp.dot(hidden, theirs, preferred_element_type=f32).astype(bf)
+        copy = remote(
+            down_send.at[part],
+            down_recv.at[part],
+            t_send.at[2 + part],
+            t_recv.at[2 + part],
+            partner,
+        )
+        copy.start()
+        swaps.append(copy)
+        mine = w_down[:, place(tp * 2 + part, quarter)]
+        kept.append(jnp.dot(hidden, mine, preferred_element_type=f32).astype(bf))
+    over = (((0,), (0,)), ((), ()))
+    middle = quarter // 2
+    return_groups = []
+    for part in range(2):
+        swaps[part].wait()
+        done = (kept[part].astype(f32) + down_recv[part].astype(f32)).astype(bf)
+        finished[part, :, :, :quarter] = done[:area].reshape(count, SUB, quarter)
+        folded = lax.dot_general(
+            lift_low, done[area:, :middle], over, preferred_element_type=f32
+        ) + lax.dot_general(lift_high, done[area:, middle:], over, preferred_element_type=f32)
+        finished[part, :, :, quarter:] = folded.astype(bf).reshape(count, SUB, middle)
+        return_groups.append(
+            scatter(finished.at[part], returned.at[part], r_send.at[part], r_recv.at[part])
+        )
+
     swap.wait()
-    done = (kept.astype(f32) + down_recv[...].astype(f32)).astype(bf)
-    finished[:, :, :half] = done[:area].reshape(count, SUB, half)
-    turn = (((0,), (0,)), ((), ()))
-    folded = lax.dot_general(
-        lift_low, done[area:, : half // 2], turn, preferred_element_type=f32
-    ) + lax.dot_general(lift_high, done[area:, half // 2 :], turn, preferred_element_type=f32)
-    finished[:, :, half:] = folded.astype(bf).reshape(count, SUB, half // 2)
-    return_copies = scatter(finished, returned, r_send, r_recv)
-    for copy in return_copies:
-        copy.wait()
-    back = returned[:, :, :half].reshape(area, half)
-    back_extra = returned[:, :, half:].reshape(area, half // 2)
+    home_columns = pl.ds(pl.multiple_of(tp * part_wide, part_wide), part_wide)
+    for owner in range(PLANE):
+        added = jnp.dot(
+            cell_mine[...], w_planes[owner, my_rows, home_columns], preferred_element_type=f32
+        ) + jnp.dot(
+            cell_theirs[...], w_planes[owner, other_rows, home_columns], preferred_element_type=f32
+        )
+        for index in range(lines // 2):
+            start = (index * PLANE + owner) * columns
+            resid[:, start : start + columns] = added[:, index * columns : (index + 1) * columns]
+    resid[...] = (tokens[:, my_half].astype(f32) + resid[...]).astype(bf).astype(f32)
+
+    @pl.loop(0, rows // 4)
+    def _(group):
+        for inner in range(4):
+            item = group * 4 + inner
+            outer = lax.dot_general(
+                left[item].astype(bf), keys[item].astype(bf), over, preferred_element_type=f32
+            ).reshape(heads, size, size)
+            new_matrix_ref[item] = decay[item][:heads][:, None, :] * matrix[item] + outer
 
     def combine(index, values):
         both = jnp.dot(chosen_in[index], values, preferred_element_type=f32)
         return both[:rows] + both[rows:]
 
-    weighted = combine(0, back) + jnp.concatenate(
-        [combine(1, back_extra), combine(2, back_extra)], axis=1
-    )
-    last_send[...] = (resid[...] + weighted).astype(bf)
-    swap = remote(last_send, last_recv, t_send.at[4], t_recv.at[4], partner)
-    swap.start()
-    mixed_ref[:, my_half] = last_send[...]
-    swap.wait()
-    mixed_ref[:, other_half] = last_recv[...]
-
-
-def update_kernel(
+    swaps = []
+    for part in range(2):
+        for group in return_groups[part].values():
+            for copy in group:
+                copy.wait()
+        back = returned[part, :, :, :quarter].reshape(area, quarter)
+        extra = returned[part, :, :, quarter:].reshape(area, middle)
+        weighted = combine(0, back) + jnp.concatenate(
+            [combine(1, extra), combine(2, extra)], axis=1
+        )
+        span = slice(part * quarter, (part + 1) * quarter)
+        last_send[part] = (resid[:, span] + weighted).astype(bf)
+        copy = remote(
+            last_send.at[part],
+            last_recv.at[part],
+            t_send.at[4 + part],
+            t_recv.at[4 + part],
+            partner,
+        )
+        copy.start()
+        swaps.append(copy)
+        mixed_ref[:, place(tp * 2 + part, quarter)] = last_send[part]
+    for part in range(2):
+        swaps[part].wait()
+        mixed_ref[:, place((1 - tp) * 2 + part, quarter)] = last_recv[part]
+
+
+def store_kernel(
     mixed_ref,
-    left_ref,
-    keys_ref,
-    decay_ref,
+    matrix_ref,
     norm_ref,
     max_ref,
-    matrix_hbm,
     mixed_out,
-    new_matrix_ref,
-    new_norm_out,
-    new_max_out,
-    matrix,
-    in_sems,
-    out_sems,
+    matrix_out,
+    norm_out,
+    max_out,
+    sems,
 ):
-    rows, heads, size, _ = matrix.shape
-    wide = heads * size
-    chunk = 8
-    chunks = rows // chunk
-    loads = []
+    chunks = 4
+    tall = matrix_ref.shape[0] // chunks
+    pairs = []
     for index in range(chunks):
-        part = pl.ds(index * chunk, chunk)
-        copy = pltpu.make_async_copy(matrix_hbm.at[part], matrix.at[part], in_sems.at[index])
-        copy.start()
-        loads.append(copy)
-    mixed_out[...] = mixed_ref[...]
-    new_norm_out[...] = norm_ref[...]
-    new_max_out[...] = max_ref[...]
-    stores = []
-    for index in range(chunks):
-        loads[index].wait()
-
-        @pl.loop(0, chunk // 4)
-        def _(group):
-            for inner in range(4):
-                item = index * chunk + group * 4 + inner
-                outer = lax.dot_general(
-                    left_ref[item].astype(jnp.bfloat16),
-                    keys_ref[item].astype(jnp.bfloat16),
-                    (((0,), (0,)), ((), ())),
-                    preferred_element_type=jnp.float32,
-                ).reshape(heads, size, size)
-                scale = decay_ref[item][:heads][:, None, :]
-                matrix[item] = scale * matrix[item] + outer
-
-        part = pl.ds(index * chunk, chunk)
-        copy = pltpu.make_async_copy(matrix.at[part], new_matrix_ref.at[part], out_sems.at[index])
-        copy.start()
-        stores.append(copy)
-    for copy in stores:
+        part = pl.ds(index * tall, tall)
+        pairs.append((matrix_ref.at[part], matrix_out.at[part]))
+    pairs += [(mixed_ref, mixed_out), (norm_ref, norm_out), (max_ref, max_out)]
+    for copy in fetch_all(pairs, sems):
         copy.wait()
 
 
@@ -787,11 +834,10 @@
     shape = jax.ShapeDtypeStruct
     tile = (count, SUB, half + half // 2)
     thin = (count, SUB, wide + wide // 2)
+    parts = (2, count, SUB, half // 2 + half // 4)
     made = (
         shape((rows, width), bf),
-        shape((rows, 2 * heads, wide), f32),
-        shape((rows, 2 * heads, size), f32),
-        shape((rows, 2 * heads, size), f32),
+        shape(state_matrix.shape, f32),
         shape(state_norm.shape, f32),
         shape((heads, rows), f32),
     )
@@ -822,7 +868,7 @@
         functools.partial(layer_kernel, count),
         out_shape=made,
         in_specs=[far] * 21,
-        out_specs=(vmem,) * 6,
+        out_specs=(vmem,) * 4,
         scratch_shapes=[
             pltpu.VMEM((rows, width), bf),
             pltpu.VMEM((1, width), f32),
@@ -867,14 +913,17 @@
             pltpu.VMEM(thin, bf),
             pltpu.VMEM((slots, width), bf),
             pltpu.VMEM((rows * 2 * heads, wide), f32),
+            pltpu.VMEM((rows, 2 * heads, wide), f32),
+            pltpu.VMEM((rows, 2 * heads, size), f32),
+            pltpu.VMEM((rows, 2 * heads, size), f32),
             pltpu.VMEM((rows, half), f32),
             pltpu.VMEM((slots, width), bf),
-            pltpu.VMEM((slots, half), bf),
-            pltpu.VMEM((slots, half), bf),
-            pltpu.VMEM(tile, bf),
-            pltpu.VMEM(tile, bf),
-            pltpu.VMEM((rows, half), bf),
-            pltpu.VMEM((rows, half), bf),
+            pltpu.VMEM((2, slots, half // 2), bf),
+            pltpu.VMEM((2, slots, half // 2), bf),
+            pltpu.VMEM(parts, bf),
+            pltpu.VMEM(parts, bf),
+            pltpu.VMEM((2, rows, half // 2), bf),
+            pltpu.VMEM((2, rows, half // 2), bf),
             dma((11,)),
             dma((6,)),
             dma((6,)),
@@ -890,35 +939,38 @@
             dma((lines,)),
             dma((lines,)),
             dma((lines,)),
+            dma((lines,)),
+            dma((lines,)),
             dma((6,)),
             dma((6,)),
-            dma((5,)),
-            dma((5,)),
+            dma((6,)),
+            dma((6,)),
             dma((count,)),
             dma((count,)),
+            dma((lines,)),
+            dma((lines,)),
             dma((count,)),
             dma((count,)),
-            dma((count,)),
-            dma((count,)),
-            dma((count,)),
-            dma((count,)),
+            dma((lines,)),
+            dma((lines,)),
+            dma((7,)),
+            dma((7,)),
+            dma((2, count)),
+            dma((2, count)),
+            pltpu.SemaphoreType.REGULAR,
         ],
         compiler_params=pltpu.CompilerParams(
             collective_id=0, has_side_effects=True, vmem_limit_bytes=LAYER_BYTES
         ),
     )(*[pltpu.with_memory_space_constraint(operand, pltpu.HBM) for operand in operands])
     mixed, new_matrix, new_norm, new_max = pl.pallas_call(
-        update_kernel,
-        out_shape=(made[0], shape(state_matrix.shape, f32), made[4], made[5]),
-        in_specs=[vmem] * 6 + [anywhere],
-        out_specs=(vmem, anywhere, vmem, vmem),
-        scratch_shapes=[
-            pltpu.VMEM(state_matrix.shape, f32),
-            dma((rows // 8,)),
-            dma((rows // 8,)),
-        ],
-        compiler_params=pltpu.CompilerParams(vmem_limit_bytes=UPDATE_BYTES),
-    )(*results, state_matrix)
+        store_kernel,
+        out_shape=made,
+        in_specs=[vmem] * 4,
+        out_specs=(anywhere,) * 4,
+        scratch_shapes=[dma((7,))],
+        compiler_params=pltpu.CompilerParams(vmem_limit_bytes=STORE_BYTES),
+    )(*results)
     return mixed, new_matrix, new_norm, jnp.swapaxes(new_max, 0, 1)
 
 

time: 58.5 us -> 55 us (0.940)
  Pallas kernels: 57.2 us -> 54.3 us
    pallas_call x1, Pallas kernels: 4.16 us -> 2.12 us  [layer_call(): pl.pallas_call(store_kernel, out_shape=made, in_specs=[vmem] * 4, out_spe...]
    pallas_call x1, Pallas kernels: 53 us -> 52.1 us  [layer_call(): pl.pallas_call(functools.partial(layer_kernel, count), out_shape=made, in...]
where the time goes in v3:
time: 55 us; the launch traced here: 54.9 us
  Pallas kernels  54.3 us (99%)
  between operations  0.65 us (1%)
    pallas_call x1, Pallas kernels, layer_call(): pl.pallas_call(functools.partial(layer_kernel, count), out_shape=made, in...  52.1 us
    pallas_call x1, Pallas kernels, layer_call(): pl.pallas_call(store_kernel, out_shape=made, in_specs=[vmem] * 4, out_spe...  2.12 us

profile of v3, /device:TPU:0, one launch (start us, length us, event | category | flops | bytes accessed | tf_op | source)
XLA Modules:
  0.0 54.9 jit_solution(3013989683508313054)
XLA Ops:
  0.6 52.1 %shard_map.228 = (bf16[32,2048]{1,0:T(8,128)(2,1)S(1)}, f32[32,4,64,64]{3,2,1,0:T(8,128)S(1)}, f32[32,4,64]{2,1,0:T(4,128)S(1)}, f32[4,32]{1,0:T(4,128)S(1)}) custom-call(bf16[32,2048]{1,0:T(8,128)(2,1)} %tokens_hbm.1, f32[1,2048]{1,0:T(1,128)} %bitcast.21, bf16[128,256]{1,0:T(8,128)(2,1)} %wq_hbm.1, bf16[128,256]{1,0:T(8,128)(2,1)} %wk_hbm.1, ...), custom_call_target="tpu_custom_call" | custom-call | tf_op jit(solution)/shard_map/pallas_call | solution.py:867
  52.8 2.1 %shard_map.229 = (bf16[32,2048]{1,0:T(8,128)(2,1)}, f32[32,4,64,64]{3,2,1,0:T(8,128)}, f32[32,4,64]{2,1,0:T(4,128)}, f32[4,32]{1,0:T(4,128)}) custom-call(bf16[32,2048]{1,0:T(8,128)(2,1)S(1)} %get-tuple-element.12.mixed_ref, f32[32,4,64,64]{3,2,1,0:T(8,128)S(1)} %get-tuple-element.13.matrix_ref, f32[32,4,64]{2,1,0:T(4,128)S(1)} %get-tuple-element.14.norm_ref, ...), custom_call_target="tpu_custom_call" | custom-call | tf_op jit(solution)/shard_map/pallas_call | solution.py:966

commit v4 on v3

--- a/solution.py
+++ b/solution.py
@@ -147,6 +147,7 @@
     left,
     keys,
     decay,
+    added,
     resid,
     row_values,
     down_send,
@@ -268,7 +269,7 @@
         return view
 
     def out_view(owner, part):
-        return w_planes.at[owner, my_rows, part * part_wide : (part + 1) * part_wide]
+        return w_planes.at[owner, my_rows, place(part, part_wide)]
 
     def open_plane(make):
         first = [
@@ -313,7 +314,7 @@
     widened = tokens[...].astype(f32)
     scale = lax.rsqrt(jnp.mean(widened * widened, axis=-1, keepdims=True) + 1e-06)
     normed[...] = (widened * scale * mix_gain[...]).astype(bf)
-    x_copies, z_copies = [], []
+    x_copies = []
     narrow = block // 2
     my_part = place(tp, narrow)
     for step in range(1, lines):
@@ -327,11 +328,18 @@
         )
         copy.start()
         x_copies.append(copy)
-    for step in range(1, lines):
-        view = w_planes.at[spot, my_rows, place(line, columns)]
-        copy = remote(view, view, z_send.at[step], z_recv.at[step], line_peer(step)[1])
+    near_line = line + 1 - 2 * (line % 2)
+    mirror_line = lines - 1 - line
+    near_peer = (near_line * PLANE + spot, tp)
+    mirror_peer = (mirror_line * PLANE + spot, tp)
+
+    def line_copy(owner, slot, target):
+        view = w_planes.at[spot, my_rows, place(owner, columns)]
+        return remote(view, view, z_send.at[slot], z_recv.at[slot], target)
+
+    z_copies = [line_copy(line, 0, near_peer), line_copy(line, 1, mirror_peer)]
+    for copy in z_copies:
         copy.start()
-        z_copies.append(copy)
     spread[line] = normed[:, place(line, block)]
     for copy in first_loads[9:]:
         copy.wait()
@@ -382,6 +390,37 @@
         )
         chosen_in[index] = joined.T[: 2 * rows].astype(bf)
 
+    line_of = (lax.rem(line + lines // 2, lines), mirror_line, near_line, line)
+    own_group = len(line_of) - 1
+
+    def scatter(groups, turns, source, near, send, recv):
+        copies = {}
+        for group in groups:
+            copies[group] = []
+            for turn in turns:
+                if group == own_group and turn == 0:
+                    near[ep] = source[ep]
+                    continue
+                other = line_of[group] * PLANE + lax.rem(spot + turn, PLANE)
+                slot = group * PLANE + turn
+                copy = remote(
+                    source.at[other], near.at[ep], send.at[slot], recv.at[slot], (other, tp)
+                )
+                copy.start()
+                copies[group].append(copy)
+        return copies
+
+    def forward(copies, near, far, send, recv):
+        passed = []
+        for group, arriving in copies.items():
+            for copy in arriving:
+                copy.wait()
+            span = place(line_of[group], PLANE)
+            copy = remote(near.at[span], far.at[span], send.at[group], recv.at[group], partner)
+            copy.start()
+            passed.append(copy)
+        return passed
+
     def pack_rows(values, target):
         middle = values.shape[1] // 2
         target[:, :, : 2 * middle] = gather_rows(chosen_out[0], values).reshape(
@@ -394,6 +433,7 @@
     a_second = relay_plane(make_a, a_first)
     b_first = open_plane(make_b)
     pack_rows(tokens[:, my_half], token_out)
+    straight_tokens = scatter(range(own_group), (0,), token_out, token_near, k_send, k_recv)
     late_loads[0].wait()
 
     def pack_matrix(start, stop):
@@ -447,11 +487,16 @@
             copies.append(copy)
         return copies
 
+    z_copies[1].wait_recv()
+    z_copies.append(line_copy(mirror_line, 2, near_peer))
+    z_copies[2].start()
     pa_copies = send_partials(outgoing_a, arrived_a, pa_send, pa_recv)
     b_second = relay_plane(make_b, b_first)
-    for copy in z_copies:
-        copy.wait()
-    o_first = open_plane(make_o)
+    z_copies[0].wait_recv()
+    held = line // (lines // 2)
+    o_first = [make_o(spot, held, 0, beside_peer), make_o(spot, held, 3, across_peer)]
+    for copy in o_first:
+        copy.start()
     slabs = []
 
     def pass_slab(view):
@@ -460,7 +505,6 @@
         copy.start()
         slabs.append(copy)
 
-    pass_slab(w_planes.at[spot, my_rows])
     pack_matrix(rows // 4, rows // 2)
     for copy in late_loads[1:7]:
         copy.wait()
@@ -499,36 +543,17 @@
     partial_b[...] = product.reshape(lines, rows, pair)
     pb_copies = send_partials(outgoing_b, arrived_b, pb_send, pb_recv)
 
-    def scatter(source, near, send, recv):
-        groups = {}
-        for hop in [lines // 2] + [n for n in range(1, lines) if n != lines // 2] + [0]:
-            groups[hop] = []
-            for turn in range(PLANE):
-                if hop == 0 and turn == 0:
-                    continue
-                other = lax.rem(line + hop, lines) * PLANE + lax.rem(spot + turn, PLANE)
-                slot = hop * PLANE + turn
-                copy = remote(
-                    source.at[other], near.at[ep], send.at[slot], recv.at[slot], (other, tp)
-                )
-                copy.start()
-                groups[hop].append(copy)
-        near[ep] = source[ep]
-        return groups
-
-    def forward(groups, near, far, send, recv):
-        copies = []
-        for hop in range(lines):
-            for copy in groups[hop]:
-                copy.wait()
-            span = place(lax.rem(line + lines - hop, lines), PLANE)
-            copy = remote(near.at[span], far.at[span], send.at[hop], recv.at[hop], partner)
-            copy.start()
-            copies.append(copy)
-        return copies
+    z_copies[2].wait_recv()
+    for copy in z_copies:
+        copy.wait_send()
 
     pl.semaphore_wait(ready, lines - 1)
-    token_copies = scatter(token_out, token_near, k_send, k_recv)
+    slanted = tuple(range(1, PLANE))
+    early_tokens = scatter((0,), slanted, token_out, token_near, k_send, k_recv)
+    o_first += [make_o(spot, 1 - held, 1, beside_peer), make_o(spot, 1 - held, 2, across_peer)]
+    for copy in o_first[2:]:
+        copy.start()
+    pass_slab(w_planes.at[spot, my_rows])
 
     total = partial_a[line]
     for step in range(1, lines):
@@ -571,9 +596,6 @@
     divisor = jnp.maximum(
         jnp.abs(keep_old * query_norm + keep_new * query_key), jnp.exp(-new_max)
     )
-    o_second = relay_plane(make_o, o_first)
-    pass_slab(out_view(beside, 0))
-    pass_slab(out_view(across, 1))
     late = partial_b[line]
     for step in range(1, lines):
         pb_copies[step - 1].wait()
@@ -590,12 +612,27 @@
     swap = remote(cell_mine, cell_theirs, t_send.at[0], t_recv.at[0], partner)
     swap.start()
     pack_rows(cell, cell_out)
-    cell_copies = scatter(cell_out, cell_near, c_send, c_recv)
-
+    everyone = range(len(line_of)), range(PLANE)
+    cell_copies = scatter(*everyone, cell_out, cell_near, c_send, c_recv)
+    late_tokens = scatter((1, 2), slanted, token_out, token_near, k_send, k_recv)
+    late_tokens.update(
+        scatter((own_group,), range(PLANE), token_out, token_near, k_send, k_recv)
+    )
+    for group in straight_tokens:
+        (early_tokens if group in early_tokens else late_tokens)[group] += straight_tokens[group]
+
+    o_first[0].wait_recv()
+    o_second = [make_o(beside, held, 4, across_peer)]
+    o_second[0].start()
+    pass_slab(out_view(beside, held))
+    o_first[1].wait_recv()
+    pass_slab(out_view(across, held))
+    o_first[3].wait_recv()
+    o_second.append(make_o(across, 1 - held, 5, beside_peer))
+    o_second[1].start()
+    pass_slab(out_view(across, 1 - held))
     o_first[2].wait_recv()
-    pass_slab(out_view(beside, 1))
-    o_first[3].wait_recv()
-    pass_slab(out_view(across, 0))
+    pass_slab(out_view(beside, 1 - held))
 
     lane_gates = gates_lane + pltpu.roll(gates_lane, LANES // 2, 1)
     lane_max, lane_old, lane_new = gate_math(
@@ -630,110 +667,147 @@
     coarse = scaled.astype(bf).astype(f32)
     left[...] = jnp.where(row < heads, coarse, scaled - coarse)
 
-    corner = PLANE - 1 - spot
-    token_forwards = forward(token_copies, token_near, token_far, kf_send, kf_recv)
-    for part in range(2):
-        o_second[part].wait_recv()
-        pass_slab(out_view(corner, part))
-
-    extra_rows = area // 2
-    lift_row = lax.broadcasted_iota(jnp.int32, (extra_rows, area), 0)
-    lift_column = lax.broadcasted_iota(jnp.int32, (extra_rows, area), 1)
+    extra_rows, block_rows = area // 4, area // 2
+    part_rows = block_rows + extra_rows
+    sides = (1 - held, held)
+    lift_row = lax.broadcasted_iota(jnp.int32, (extra_rows, block_rows), 0)
+    lift_column = lax.broadcasted_iota(jnp.int32, (extra_rows, block_rows), 1)
     lift_place = (lift_row // (SUB // 2)) * SUB + lift_row % (SUB // 2)
     lift_low = ones_where(lift_column == lift_place)
     lift_high = ones_where(lift_column == lift_place + SUB // 2)
 
     def unpack_rows(source):
         middle = source.shape[2] // 3
-        flat = source[:, :, : 2 * middle].reshape(area, 2 * middle)
-        extra = source[:, :, 2 * middle :].reshape(area, middle)
-        joined = jnp.concatenate(
-            [gather_rows(lift_low, extra), gather_rows(lift_high, extra)], axis=1
-        )
-        return jnp.concatenate([flat, joined], axis=0)
-
-    token_rows[:, my_half] = unpack_rows(token_near)
-    for copy in token_forwards:
-        copy.wait()
-    token_rows[:, other_half] = unpack_rows(token_far)
-
+        pieces = []
+        for side in sides:
+            span = place(side, count // 2)
+            extra = source[span, :, 2 * middle :].reshape(block_rows, middle)
+            pieces.append(source[span, :, : 2 * middle].reshape(block_rows, 2 * middle))
+            pieces.append(
+                jnp.concatenate(
+                    [gather_rows(lift_low, extra), gather_rows(lift_high, extra)], axis=1
+                )
+            )
+        return jnp.concatenate(pieces, axis=0)
+
+    token_forwards = forward(early_tokens, token_near, token_far, kf_send, kf_recv)
+    corner = PLANE - 1 - spot
+    for part in range(2):
+        o_second[part].wait_recv()
+        pass_slab(out_view(corner, held if part == 0 else 1 - held))
     forwards = forward(cell_copies, cell_near, cell_far, f_send, f_recv)
     near_rows = unpack_rows(cell_near)
     for copy in o_first + o_second:
         copy.wait_send()
-    near_parts = [
-        jnp.dot(near_rows, w_planes[owner, my_rows], preferred_element_type=f32)
-        for owner in range(PLANE)
-    ]
+    for owner in range(PLANE):
+        added[owner] = jnp.dot(near_rows, w_planes[owner, my_rows], preferred_element_type=f32)
+    token_forwards += forward(late_tokens, token_near, token_far, kf_send, kf_recv)
     for copy in slabs:
         copy.wait()
     for copy in forwards:
         copy.wait()
     far_rows = unpack_rows(cell_far)
-    squares = jnp.zeros((near_rows.shape[0], columns), f32)
     for owner in range(PLANE):
-        added = near_parts[owner] + jnp.dot(
-            far_rows, w_planes[owner, other_rows], preferred_element_type=f32
-        )
-        for index in range(lines):
-            start = (index * PLANE + owner) * columns
-            place_columns = slice(start, start + columns)
-            summed = (
-                token_rows[:, place_columns].astype(f32)
-                + added[:, index * columns : (index + 1) * columns]
-            ).astype(bf)
-            row_values[:, place_columns] = summed
-            widened = summed.astype(f32)
-            squares += widened * widened
-    scale = lax.rsqrt(jnp.sum(squares, axis=-1, keepdims=True) * (1.0 / width) + 1e-06)
-    row_values[...] = (row_values[...].astype(f32) * scale * ffn_gain[...]).astype(bf)
+        added[owner] += jnp.dot(far_rows, w_planes[owner, other_rows], preferred_element_type=f32)
+    token_rows[:, my_half] = unpack_rows(token_near)
+    for copy in token_forwards:
+        copy.wait()
+    token_rows[:, other_half] = unpack_rows(token_far)
     for copy in late_loads[7:]:
         copy.wait()
-    gate_pre = dot_t(row_values[...], w_gate[...])
-    up_pre = dot_t(row_values[...], w_up[...])
-    hidden = (gate_pre * jax.nn.sigmoid(gate_pre) * up_pre).astype(bf)
     quarter = half // 2
-    swaps, kept = [], []
-    for part in range(2):
-        theirs = w_down[:, place((1 - tp) * 2 + part, quarter)]
-        down_send[part] = jnp.dot(hidden, theirs, preferred_element_type=f32).astype(bf)
-        copy = remote(
-            down_send.at[part],
-            down_recv.at[part],
-            t_send.at[2 + part],
-            t_recv.at[2 + part],
-            partner,
-        )
-        copy.start()
-        swaps.append(copy)
-        mine = w_down[:, place(tp * 2 + part, quarter)]
-        kept.append(jnp.dot(hidden, mine, preferred_element_type=f32).astype(bf))
+    middle = quarter // 2
     over = (((0,), (0,)), ((), ()))
-    middle = quarter // 2
-    return_groups = []
-    for part in range(2):
-        swaps[part].wait()
-        done = (kept[part].astype(f32) + down_recv[part].astype(f32)).astype(bf)
-        finished[part, :, :, :quarter] = done[:area].reshape(count, SUB, quarter)
-        folded = lax.dot_general(
-            lift_low, done[area:, :middle], over, preferred_element_type=f32
-        ) + lax.dot_general(lift_high, done[area:, middle:], over, preferred_element_type=f32)
-        finished[part, :, :, quarter:] = folded.astype(bf).reshape(count, SUB, middle)
-        return_groups.append(
-            scatter(finished.at[part], returned.at[part], r_send.at[part], r_recv.at[part])
-        )
+
+    def raw_rows(index):
+        span = slice(index * part_rows, (index + 1) * part_rows)
+        squares = jnp.zeros((part_rows, columns), f32)
+        for owner in range(PLANE):
+            for step in range(lines):
+                start = (step * PLANE + owner) * columns
+                across_columns = slice(start, start + columns)
+                summed = (
+                    token_rows[span, across_columns].astype(f32)
+                    + added[owner, span, step * columns : (step + 1) * columns]
+                )
+                widened = summed.astype(bf).astype(f32)
+                row_values[span, across_columns] = (
+                    widened * ffn_gain[:, across_columns]
+                ).astype(bf)
+                squares += widened * widened
+        return squares
+
+    def run_expert(index, squares):
+        span = slice(index * part_rows, (index + 1) * part_rows)
+        values = row_values[span, :]
+        gate_pre = dot_t(values, w_gate[...])
+        up_pre = dot_t(values, w_up[...])
+        scale = lax.rsqrt(jnp.sum(squares, axis=-1, keepdims=True) * (1.0 / width) + 1e-06)
+        gate_pre, up_pre = gate_pre * scale, up_pre * scale
+        hidden = (gate_pre * jax.nn.sigmoid(gate_pre) * up_pre).astype(bf)
+        swaps, kept = [], []
+        for part in range(2):
+            theirs = w_down[:, place((1 - tp) * 2 + part, quarter)]
+            down_send[index, part] = jnp.dot(hidden, theirs, preferred_element_type=f32).astype(bf)
+            slot = 2 + 2 * index + part
+            copy = remote(
+                down_send.at[index, part],
+                down_recv.at[index, part],
+                t_send.at[slot],
+                t_recv.at[slot],
+                partner,
+            )
+            copy.start()
+            swaps.append(copy)
+            mine = w_down[:, place(tp * 2 + part, quarter)]
+            kept.append(jnp.dot(hidden, mine, preferred_element_type=f32).astype(bf))
+        return swaps, kept
+
+    def send_back(index, swaps, kept):
+        span = place(sides[index], count // 2)
+        groups = ((0, 1), (2, 3))[index]
+        for part in range(2):
+            swaps[part].wait()
+            done = (kept[part].astype(f32) + down_recv[index, part].astype(f32)).astype(bf)
+            finished[part, span, :, :quarter] = done[:block_rows].reshape(
+                count // 2, SUB, quarter
+            )
+            folded = lax.dot_general(
+                lift_low, done[block_rows:, :middle], over, preferred_element_type=f32
+            ) + lax.dot_general(
+                lift_high, done[block_rows:, middle:], over, preferred_element_type=f32
+            )
+            finished[part, span, :, quarter:] = folded.astype(bf).reshape(
+                count // 2, SUB, middle
+            )
+            return_copies[part].update(
+                scatter(
+                    groups,
+                    range(PLANE),
+                    finished.at[part],
+                    returned.at[part],
+                    r_send.at[part],
+                    r_recv.at[part],
+                )
+            )
+
+    return_copies = [{}, {}]
+    pending = run_expert(0, raw_rows(0))
+    squares = raw_rows(1)
+    send_back(0, *pending)
+    send_back(1, *run_expert(1, squares))
 
     swap.wait()
     home_columns = pl.ds(pl.multiple_of(tp * part_wide, part_wide), part_wide)
     for owner in range(PLANE):
-        added = jnp.dot(
+        shared = jnp.dot(
             cell_mine[...], w_planes[owner, my_rows, home_columns], preferred_element_type=f32
         ) + jnp.dot(
             cell_theirs[...], w_planes[owner, other_rows, home_columns], preferred_element_type=f32
         )
         for index in range(lines // 2):
             start = (index * PLANE + owner) * columns
-            resid[:, start : start + columns] = added[:, index * columns : (index + 1) * columns]
+            resid[:, start : start + columns] = shared[:, index * columns : (index + 1) * columns]
     resid[...] = (tokens[:, my_half].astype(f32) + resid[...]).astype(bf).astype(f32)
 
     @pl.loop(0, rows // 4)
@@ -751,7 +825,7 @@
 
     swaps = []
     for part in range(2):
-        for group in return_groups[part].values():
+        for group in return_copies[part].values():
             for copy in group:
                 copy.wait()
         back = returned[part, :, :, :quarter].reshape(area, quarter)
@@ -764,8 +838,8 @@
         copy = remote(
             last_send.at[part],
             last_recv.at[part],
-            t_send.at[4 + part],
-            t_recv.at[4 + part],
+            t_send.at[6 + part],
+            t_recv.at[6 + part],
             partner,
         )
         copy.start()
@@ -916,10 +990,11 @@
             pltpu.VMEM((rows, 2 * heads, wide), f32),
             pltpu.VMEM((rows, 2 * heads, size), f32),
             pltpu.VMEM((rows, 2 * heads, size), f32),
+            pltpu.VMEM((PLANE, slots, width // PLANE), f32),
             pltpu.VMEM((rows, half), f32),
             pltpu.VMEM((slots, width), bf),
-            pltpu.VMEM((2, slots, half // 2), bf),
-            pltpu.VMEM((2, slots, half // 2), bf),
+            pltpu.VMEM((2, 2, slots // 2, half // 2), bf),
+            pltpu.VMEM((2, 2, slots // 2, half // 2), bf),
             pltpu.VMEM(parts, bf),
             pltpu.VMEM(parts, bf),
             pltpu.VMEM((2, rows, half // 2), bf),
@@ -943,8 +1018,8 @@
             dma((lines,)),
             dma((6,)),
             dma((6,)),
-            dma((6,)),
-            dma((6,)),
+            dma((8,)),
+            dma((8,)),
             dma((count,)),
             dma((count,)),
             dma((lines,)),
@@ -1040,6 +1115,7 @@
         and w_expert_gate.shape[0] == 1
         and capacity == SUB + SUB // 2
         and ep_count * SUB == LANES
+        and ep_count // PLANE == 4
         and w_query.shape[1] == 2 * LANES
     )
 

time: 55 us -> 53.3 us (0.969)
  Pallas kernels: 54.3 us -> 52.5 us
    pallas_call x1, Pallas kernels: 52.1 us -> 50.4 us  [layer_call(): pl.pallas_call(functools.partial(layer_kernel, count), out_shape=made, in...]
where the time goes in v4:
time: 53.3 us; the launch traced here: 53.2 us
  Pallas kernels  52.5 us (98%)
  between operations  0.65 us (1%)
    pallas_call x1, Pallas kernels, layer_call(): pl.pallas_call(functools.partial(layer_kernel, count), out_shape=made, in...  50.4 us
    pallas_call x1, Pallas kernels, layer_call(): pl.pallas_call(store_kernel, out_shape=made, in_specs=[vmem] * 4, out_spe...  2.12 us

profile of v4, /device:TPU:0, one launch (start us, length us, event | category | flops | bytes accessed | tf_op | source)
XLA Modules:
  0.0 53.2 jit_solution(1450935395649934992)
XLA Ops:
  0.6 50.4 %shard_map.228 = (bf16[32,2048]{1,0:T(8,128)(2,1)S(1)}, f32[32,4,64,64]{3,2,1,0:T(8,128)S(1)}, f32[32,4,64]{2,1,0:T(4,128)S(1)}, f32[4,32]{1,0:T(4,128)S(1)}) custom-call(bf16[32,2048]{1,0:T(8,128)(2,1)} %tokens_hbm.1, f32[1,2048]{1,0:T(1,128)} %bitcast.21, bf16[128,256]{1,0:T(8,128)(2,1)} %wq_hbm.1, bf16[128,256]{1,0:T(8,128)(2,1)} %wk_hbm.1, ...), custom_call_target="tpu_custom_call" | custom-call | tf_op jit(solution)/shard_map/pallas_call | solution.py:941
  51.1 2.1 %shard_map.229 = (bf16[32,2048]{1,0:T(8,128)(2,1)}, f32[32,4,64,64]{3,2,1,0:T(8,128)}, f32[32,4,64]{2,1,0:T(4,128)}, f32[4,32]{1,0:T(4,128)}) custom-call(bf16[32,2048]{1,0:T(8,128)(2,1)S(1)} %get-tuple-element.12.mixed_ref, f32[32,4,64,64]{3,2,1,0:T(8,128)S(1)} %get-tuple-element.13.matrix_ref, f32[32,4,64]{2,1,0:T(4,128)S(1)} %get-tuple-element.14.norm_ref, ...), custom_call_target="tpu_custom_call" | custom-call | tf_op jit(solution)/shard_map/pallas_call | solution.py:1041

commit v5 on v4

--- a/solution.py
+++ b/solution.py
@@ -155,8 +155,10 @@
     finished,
     returned,
     last_send,
-    last_recv,
+    norm_made,
+    max_made,
     local_sem,
+    store_sem,
     a_send,
     a_recv,
     b_send,
@@ -177,12 +179,8 @@
     o_recv,
     t_send,
     t_recv,
-    k_send,
-    k_recv,
     kf_send,
     kf_recv,
-    c_send,
-    c_recv,
     f_send,
     f_recv,
     w_send,
@@ -254,10 +252,13 @@
     for step in range(1, lines):
         pl.semaphore_signal(ready, inc=1, device_id=line_peer(step)[1], device_id_type=MESH)
 
-    def plane_copies(buffer_view, send, recv):
+    def all_of(view, send, recv):
+        return remote(view, view, send.at[0], recv, partner)
+
+    def plane_copies(buffer_view, send, recv, kept=2):
         def make(owner, part, slot, target):
             view = buffer_view(owner, part)
-            return remote(view, view, send.at[slot], recv.at[slot], target)
+            return remote(view, view, send.at[0], recv.at[min(slot, kept)], target)
 
         return make
 
@@ -274,8 +275,8 @@
     def open_plane(make):
         first = [
             make(spot, 0, 0, beside_peer),
-            make(spot, 1, 2, across_peer),
-            make(spot, 1, 1, beside_peer),
+            make(spot, 1, 1, across_peer),
+            make(spot, 1, 2, beside_peer),
             make(spot, 0, 3, across_peer),
         ]
         for copy in first:
@@ -289,26 +290,18 @@
         first[1].wait_recv()
         aside = make(across, 1, 5, beside_peer)
         aside.start()
-        return [ahead, aside]
-
-    def close_plane(first, second):
-        first[2].wait_recv()
-        first[3].wait_recv()
-        for copy in first:
-            copy.wait_send()
-        for copy in second:
-            copy.wait()
+
+    def close_plane(buffer, send, recv):
+        all_of(buffer.at[pl.ds(0, 2 * depth)], send, recv.at[2]).wait_recv()
+        all_of(buffer.at[pl.ds(0, 3 * depth)], send, recv.at[2]).wait_send()
 
     make_a = plane_copies(weight_view(weights_a), a_send, a_recv)
     make_b = plane_copies(weight_view(weights_b), b_send, b_recv)
-    make_o = plane_copies(out_view, o_send, o_recv)
+    make_o = plane_copies(out_view, o_send, o_recv, 5)
     a_first = open_plane(make_a)
-    gate_copies = []
-    for slot, target in enumerate((beside_peer, across_peer, corner_peer)):
+    for target in (beside_peer, across_peer, corner_peer):
         view = gate_rows.at[spot]
-        copy = remote(view, view, g_send.at[slot], g_recv.at[slot], target)
-        copy.start()
-        gate_copies.append(copy)
+        remote(view, view, g_send.at[0], g_recv.at[0], target).start()
     for copy in first_loads[4:9]:
         copy.wait()
     widened = tokens[...].astype(f32)
@@ -322,8 +315,8 @@
         copy = remote(
             normed.at[:, place(other * 2 + tp, narrow)],
             spread.at[line, :, my_part],
-            x_send.at[step],
-            x_recv.at[step],
+            x_send.at[0],
+            x_recv.at[step - 1],
             target,
         )
         copy.start()
@@ -335,7 +328,7 @@
 
     def line_copy(owner, slot, target):
         view = w_planes.at[spot, my_rows, place(owner, columns)]
-        return remote(view, view, z_send.at[slot], z_recv.at[slot], target)
+        return remote(view, view, z_send.at[0], z_recv.at[slot], target)
 
     z_copies = [line_copy(line, 0, near_peer), line_copy(line, 1, mirror_peer)]
     for copy in z_copies:
@@ -392,34 +385,37 @@
 
     line_of = (lax.rem(line + lines // 2, lines), mirror_line, near_line, line)
     own_group = len(line_of) - 1
-
-    def scatter(groups, turns, source, near, send, recv):
-        copies = {}
+    spot_of = (spot, beside, across, PLANE - 1 - spot)
+
+    def scatter(groups, turns, source, near, family):
         for group in groups:
-            copies[group] = []
             for turn in turns:
                 if group == own_group and turn == 0:
                     near[ep] = source[ep]
                     continue
-                other = line_of[group] * PLANE + lax.rem(spot + turn, PLANE)
-                slot = group * PLANE + turn
-                copy = remote(
-                    source.at[other], near.at[ep], send.at[slot], recv.at[slot], (other, tp)
-                )
-                copy.start()
-                copies[group].append(copy)
-        return copies
-
-    def forward(copies, near, far, send, recv):
-        passed = []
-        for group, arriving in copies.items():
-            for copy in arriving:
-                copy.wait()
+                other = line_of[group] * PLANE + spot_of[turn]
+                remote(
+                    source.at[other],
+                    near.at[ep],
+                    r_send.at[family],
+                    r_recv.at[family, group],
+                    (other, tp),
+                ).start()
+
+    def wait_group(group, near, family):
+        span = pl.ds(0, PLANE - 1) if group == own_group else place(line_of[group], PLANE)
+        view = near.at[span]
+        remote(view, view, r_send.at[family], r_recv.at[family, group], partner).wait_recv()
+
+    def wait_sent(source, family):
+        view = source.at[pl.ds(0, count - 1)]
+        remote(view, view, r_send.at[family], r_recv.at[family, 0], partner).wait_send()
+
+    def forward(groups, near, far, family, send, recv):
+        for group in groups:
+            wait_group(group, near, family)
             span = place(line_of[group], PLANE)
-            copy = remote(near.at[span], far.at[span], send.at[group], recv.at[group], partner)
-            copy.start()
-            passed.append(copy)
-        return passed
+            remote(near.at[span], far.at[span], send.at[0], recv.at[0], partner).start()
 
     def pack_rows(values, target):
         middle = values.shape[1] // 2
@@ -430,10 +426,10 @@
         extra += jnp.dot(chosen_out[2], values[:, middle:], preferred_element_type=f32)
         target[:, :, 2 * middle :] = extra.astype(bf).reshape(count, SUB, middle)
 
-    a_second = relay_plane(make_a, a_first)
+    relay_plane(make_a, a_first)
     b_first = open_plane(make_b)
     pack_rows(tokens[:, my_half], token_out)
-    straight_tokens = scatter(range(own_group), (0,), token_out, token_near, k_send, k_recv)
+    scatter(range(own_group), (0,), token_out, token_near, 0)
     late_loads[0].wait()
 
     def pack_matrix(start, stop):
@@ -448,23 +444,20 @@
             packed[index, : 2 * size] = upper
             packed[index, 2 * size :] = (flipped - upper.astype(f32)).astype(bf)
 
-    y_copies = []
     for step in range(1, lines):
-        x_copies[step - 1].wait()
+        x_copies[step - 1].wait_recv()
         view = spread.at[lax.rem(line + lines - step, lines), :, my_part]
-        copy = remote(view, view, y_send.at[step], y_recv.at[step], partner)
-        copy.start()
-        y_copies.append(copy)
+        remote(view, view, y_send.at[0], y_recv.at[0], partner).start()
     pack_matrix(0, rows // 4)
-    for copy in gate_copies:
-        copy.wait()
+    all_of(gate_rows.at[pl.ds(0, PLANE - 1)], g_send, g_recv.at[0]).wait()
     for owner in range(PLANE):
         part = gate_rows[owner]
         gate_t[: 2 * heads, owner * depth : (owner + 1) * depth] = part
         gate_t[LANES // 2 : LANES // 2 + 2 * heads, owner * depth : (owner + 1) * depth] = part
-    for copy in y_copies:
-        copy.wait()
-    close_plane(a_first, a_second)
+    others = pl.ds(1, lines - 1)
+    all_of(spread.at[others, :, my_part], x_send, x_recv.at[0]).wait_send()
+    all_of(spread.at[others, :, my_part], y_send, y_recv.at[0]).wait()
+    close_plane(weights_a, a_send, a_recv)
     arranged = spread[...].reshape(lines * rows, block)
     product = jnp.dot(arranged, weights_a[...], preferred_element_type=f32)
     gates = dot_t(arranged, gate_t[...])
@@ -477,33 +470,25 @@
     partial_a[:, :, pair:] = jnp.where(first, gates, 0.0).reshape(lines, rows, LANES)
 
     def send_partials(outgoing, arrived, send, recv):
-        copies = []
         for step in range(1, lines):
             other, target = line_peer(step)
-            copy = remote(
-                outgoing.at[other], arrived.at[step], send.at[step], recv.at[step], target
-            )
-            copy.start()
-            copies.append(copy)
-        return copies
+            remote(
+                outgoing.at[other], arrived.at[step], send.at[0], recv.at[0], target
+            ).start()
 
     z_copies[1].wait_recv()
     z_copies.append(line_copy(mirror_line, 2, near_peer))
     z_copies[2].start()
-    pa_copies = send_partials(outgoing_a, arrived_a, pa_send, pa_recv)
-    b_second = relay_plane(make_b, b_first)
+    send_partials(outgoing_a, arrived_a, pa_send, pa_recv)
+    relay_plane(make_b, b_first)
     z_copies[0].wait_recv()
     held = line // (lines // 2)
     o_first = [make_o(spot, held, 0, beside_peer), make_o(spot, held, 3, across_peer)]
     for copy in o_first:
         copy.start()
-    slabs = []
 
     def pass_slab(view):
-        slot = len(slabs)
-        copy = remote(view, view, w_send.at[slot], w_recv.at[slot], partner)
-        copy.start()
-        slabs.append(copy)
+        remote(view, view, w_send.at[0], w_recv.at[0], partner).start()
 
     pack_matrix(rows // 4, rows // 2)
     for copy in late_loads[1:7]:
@@ -537,27 +522,27 @@
     )
     old_norm = jnp.concatenate([state_norm[:, head, :] for head in range(heads)], axis=1)
 
-    close_plane(b_first, b_second)
+    close_plane(weights_b, b_send, b_recv)
     product = jnp.dot(arranged, weights_b[...], preferred_element_type=f32)
     outgoing_b[...] = product.astype(bf).reshape(lines, rows, pair)
     partial_b[...] = product.reshape(lines, rows, pair)
-    pb_copies = send_partials(outgoing_b, arrived_b, pb_send, pb_recv)
+    send_partials(outgoing_b, arrived_b, pb_send, pb_recv)
 
     z_copies[2].wait_recv()
-    for copy in z_copies:
-        copy.wait_send()
+    all_of(w_planes.at[spot, my_rows, pl.ds(0, 3 * columns)], z_send, z_recv.at[0]).wait_send()
 
     pl.semaphore_wait(ready, lines - 1)
-    slanted = tuple(range(1, PLANE))
-    early_tokens = scatter((0,), slanted, token_out, token_near, k_send, k_recv)
+    slanted = tuple(range(PLANE - 1, 0, -1))
+    scatter((0, own_group), slanted, token_out, token_near, 0)
+    token_near[ep] = token_out[ep]
     o_first += [make_o(spot, 1 - held, 1, beside_peer), make_o(spot, 1 - held, 2, across_peer)]
     for copy in o_first[2:]:
         copy.start()
     pass_slab(w_planes.at[spot, my_rows])
 
     total = partial_a[line]
+    all_of(arrived_a.at[others], pa_send, pa_recv.at[0]).wait()
     for step in range(1, lines):
-        pa_copies[step - 1].wait()
         total = total + arrived_a[step].astype(f32)
     gates_lane = total[:, pair:]
     gates_wide = exact_dot([gates_lane], chosen_head)[0]
@@ -597,8 +582,8 @@
         jnp.abs(keep_old * query_norm + keep_new * query_key), jnp.exp(-new_max)
     )
     late = partial_b[line]
+    all_of(arrived_b.at[others], pb_send, pb_recv.at[0]).wait()
     for step in range(1, lines):
-        pb_copies[step - 1].wait()
         late = late + arrived_b[step].astype(f32)
     value = late[:, :wide].astype(bf).astype(f32)
     outgate = late[:, wide:].astype(bf).astype(f32)
@@ -612,15 +597,9 @@
     swap = remote(cell_mine, cell_theirs, t_send.at[0], t_recv.at[0], partner)
     swap.start()
     pack_rows(cell, cell_out)
-    everyone = range(len(line_of)), range(PLANE)
-    cell_copies = scatter(*everyone, cell_out, cell_near, c_send, c_recv)
-    late_tokens = scatter((1, 2), slanted, token_out, token_near, k_send, k_recv)
-    late_tokens.update(
-        scatter((own_group,), range(PLANE), token_out, token_near, k_send, k_recv)
-    )
-    for group in straight_tokens:
-        (early_tokens if group in early_tokens else late_tokens)[group] += straight_tokens[group]
-
+    everyone = range(len(line_of))
+    scatter(everyone, slanted + (0,), cell_out, cell_near, 1)
+    scatter((1, 2), slanted, token_out, token_near, 0)
     o_first[0].wait_recv()
     o_second = [make_o(beside, held, 4, across_peer)]
     o_second[0].start()
@@ -641,7 +620,7 @@
         old_max_lane,
     )
     turned[:rows, :] = lane_max
-    new_max_ref[...] = turned[...].T[:heads, :rows]
+    max_made[...] = turned[...].T[:heads, :rows]
     row_lane = lax.broadcasted_iota(jnp.int32, (rows, pack, LANES), 1)
     lane = lax.broadcasted_iota(jnp.int32, (rows, pack, LANES), 2)
     chosen = ((row_lane == lane) | (row_lane == lane + heads)) & (lane < heads)
@@ -660,12 +639,13 @@
         preferred_element_type=f32,
     ).reshape(rows, pack, size)
     keys[...] = key_rows
-    new_norm_ref[...] = (
+    norm_made[...] = (
         old_scale[:, :heads] * state_norm[...] + (new_scale * key_rows)[:, :heads]
     )
     scaled = jnp.where(same, jnp.broadcast_to(value[:, None, :], same.shape) * new_scale, 0.0)
     coarse = scaled.astype(bf).astype(f32)
     left[...] = jnp.where(row < heads, coarse, scaled - coarse)
+    stores = fetch_all(((norm_made, new_norm_ref), (max_made, new_max_ref)), store_sem)
 
     extra_rows, block_rows = area // 4, area // 2
     part_rows = block_rows + extra_rows
@@ -690,28 +670,24 @@
             )
         return jnp.concatenate(pieces, axis=0)
 
-    token_forwards = forward(early_tokens, token_near, token_far, kf_send, kf_recv)
+    forward((0, own_group), token_near, token_far, 0, kf_send, kf_recv)
     corner = PLANE - 1 - spot
     for part in range(2):
         o_second[part].wait_recv()
         pass_slab(out_view(corner, held if part == 0 else 1 - held))
-    forwards = forward(cell_copies, cell_near, cell_far, f_send, f_recv)
+    forward(everyone, cell_near, cell_far, 1, f_send, f_recv)
     near_rows = unpack_rows(cell_near)
-    for copy in o_first + o_second:
-        copy.wait_send()
+    all_of(w_planes.at[pl.ds(0, PLANE - 1), my_rows], o_send, o_recv.at[0]).wait_send()
     for owner in range(PLANE):
         added[owner] = jnp.dot(near_rows, w_planes[owner, my_rows], preferred_element_type=f32)
-    token_forwards += forward(late_tokens, token_near, token_far, kf_send, kf_recv)
-    for copy in slabs:
-        copy.wait()
-    for copy in forwards:
-        copy.wait()
+    forward((1, 2), token_near, token_far, 0, kf_send, kf_recv)
+    token_rows[:, my_half] = unpack_rows(token_near)
+    all_of(w_planes.at[:, my_rows], w_send, w_recv.at[0]).wait()
+    all_of(cell_near, f_send, f_recv.at[0]).wait()
     far_rows = unpack_rows(cell_far)
     for owner in range(PLANE):
         added[owner] += jnp.dot(far_rows, w_planes[owner, other_rows], preferred_element_type=f32)
-    token_rows[:, my_half] = unpack_rows(token_near)
-    for copy in token_forwards:
-        copy.wait()
+    all_of(token_near, kf_send, kf_recv.at[0]).wait()
     token_rows[:, other_half] = unpack_rows(token_far)
     for copy in late_loads[7:]:
         copy.wait()
@@ -749,7 +725,7 @@
         for part in range(2):
             theirs = w_down[:, place((1 - tp) * 2 + part, quarter)]
             down_send[index, part] = jnp.dot(hidden, theirs, preferred_element_type=f32).astype(bf)
-            slot = 2 + 2 * index + part
+            slot = 1 + 2 * index + part
             copy = remote(
                 down_send.at[index, part],
                 down_recv.at[index, part],
@@ -780,24 +756,16 @@
             finished[part, span, :, quarter:] = folded.astype(bf).reshape(
                 count // 2, SUB, middle
             )
-            return_copies[part].update(
-                scatter(
-                    groups,
-                    range(PLANE),
-                    finished.at[part],
-                    returned.at[part],
-                    r_send.at[part],
-                    r_recv.at[part],
-                )
-            )
-
-    return_copies = [{}, {}]
+            scatter(groups, slanted + (0,), finished.at[part], returned.at[part], 2 + part)
+
     pending = run_expert(0, raw_rows(0))
     squares = raw_rows(1)
     send_back(0, *pending)
     send_back(1, *run_expert(1, squares))
 
     swap.wait()
+    wait_sent(token_out, 0)
+    wait_sent(cell_out, 1)
     home_columns = pl.ds(pl.multiple_of(tp * part_wide, part_wide), part_wide)
     for owner in range(PLANE):
         shared = jnp.dot(
@@ -817,7 +785,11 @@
             outer = lax.dot_general(
                 left[item].astype(bf), keys[item].astype(bf), over, preferred_element_type=f32
             ).reshape(heads, size, size)
-            new_matrix_ref[item] = decay[item][:heads][:, None, :] * matrix[item] + outer
+            matrix[item] = decay[item][:heads][:, None, :] * matrix[item] + outer
+
+    store = pltpu.make_async_copy(matrix, new_matrix_ref, store_sem.at[2])
+    store.start()
+    stores.append(store)
 
     def combine(index, values):
         both = jnp.dot(chosen_in[index], values, preferred_element_type=f32)
@@ -825,9 +797,8 @@
 
     swaps = []
     for part in range(2):
-        for group in return_copies[part].values():
-            for copy in group:
-                copy.wait()
+        for group in everyone:
+            wait_group(group, returned.at[part], 2 + part)
         back = returned[part, :, :, :quarter].reshape(area, quarter)
         extra = returned[part, :, :, quarter:].reshape(area, middle)
         weighted = combine(0, back) + jnp.concatenate(
@@ -835,19 +806,19 @@
         )
         span = slice(part * quarter, (part + 1) * quarter)
         last_send[part] = (resid[:, span] + weighted).astype(bf)
+        target = mixed_ref.at[:, place(tp * 2 + part, quarter)]
         copy = remote(
-            last_send.at[part],
-            last_recv.at[part],
-            t_send.at[6 + part],
-            t_recv.at[6 + part],
-            partner,
+            last_send.at[part], target, t_send.at[5 + part], t_recv.at[5 + part], partner
         )
         copy.start()
         swaps.append(copy)
-        mixed_ref[:, place(tp * 2 + part, quarter)] = last_send[part]
+        store = pltpu.make_async_copy(last_send.at[part], target, store_sem.at[3 + part])
+        store.start()
+        stores.append(store)
     for part in range(2):
-        swaps[part].wait()
-        mixed_ref[:, place((1 - tp) * 2 + part, quarter)] = last_recv[part]
+        wait_sent(finished.at[part], 2 + part)
+    for copy in stores + swaps:
+        copy.wait()
 
 
 def store_kernel(
@@ -940,9 +911,9 @@
     )
     results = pl.pallas_call(
         functools.partial(layer_kernel, count),
-        out_shape=made,
+        out_shape=tuple(pltpu.VMEM(each.shape, each.dtype) for each in made),
         in_specs=[far] * 21,
-        out_specs=(vmem,) * 4,
+        out_specs=(anywhere,) * 4,
         scratch_shapes=[
             pltpu.VMEM((rows, width), bf),
             pltpu.VMEM((1, width), f32),
@@ -998,40 +969,38 @@
             pltpu.VMEM(parts, bf),
             pltpu.VMEM(parts, bf),
             pltpu.VMEM((2, rows, half // 2), bf),
-            pltpu.VMEM((2, rows, half // 2), bf),
+            pltpu.VMEM(state_norm.shape, f32),
+            pltpu.VMEM((heads, rows), f32),
             dma((11,)),
+            dma((5,)),
+            dma((1,)),
+            dma((3,)),
+            dma((1,)),
+            dma((3,)),
+            dma((1,)),
+            dma((1,)),
+            dma((1,)),
+            dma((lines - 1,)),
+            dma((1,)),
+            dma((1,)),
+            dma((1,)),
+            dma((lines - 1,)),
+            dma((1,)),
+            dma((1,)),
+            dma((1,)),
+            dma((1,)),
+            dma((1,)),
             dma((6,)),
-            dma((6,)),
-            dma((6,)),
-            dma((6,)),
-            dma((3,)),
-            dma((3,)),
-            dma((lines,)),
-            dma((lines,)),
-            dma((lines,)),
-            dma((lines,)),
-            dma((lines,)),
-            dma((lines,)),
-            dma((lines,)),
-            dma((lines,)),
-            dma((lines,)),
-            dma((lines,)),
-            dma((6,)),
-            dma((6,)),
-            dma((8,)),
-            dma((8,)),
-            dma((count,)),
-            dma((count,)),
-            dma((lines,)),
-            dma((lines,)),
-            dma((count,)),
-            dma((count,)),
-            dma((lines,)),
-            dma((lines,)),
             dma((7,)),
             dma((7,)),
-            dma((2, count)),
-            dma((2, count)),
+            dma((1,)),
+            dma((1,)),
+            dma((1,)),
+            dma((1,)),
+            dma((1,)),
+            dma((1,)),
+            dma((4,)),
+            dma((4, lines)),
             pltpu.SemaphoreType.REGULAR,
         ],
         compiler_params=pltpu.CompilerParams(
@@ -1041,7 +1010,7 @@
     mixed, new_matrix, new_norm, new_max = pl.pallas_call(
         store_kernel,
         out_shape=made,
-        in_specs=[vmem] * 4,
+        in_specs=[anywhere] * 4,
         out_specs=(anywhere,) * 4,
         scratch_shapes=[dma((7,))],
         compiler_params=pltpu.CompilerParams(vmem_limit_bytes=STORE_BYTES),

time: 53.3 us -> 51 us (0.957)
  Pallas kernels: 52.5 us -> 50.2 us
    pallas_call x2, Pallas kernels: 52.5 us -> 50.2 us  [the longest x1 48 us: layer_call(): pl.pallas_call(functools.partial(layer_kernel, count), out_shape=tuple((p...]
where the time goes in v5:
time: 51 us; the launch traced here: 50.8 us
  Pallas kernels  50.2 us (98%)
  between operations  0.65 us (1%)
    pallas_call x1, Pallas kernels, layer_call(): pl.pallas_call(functools.partial(layer_kernel, count), out_shape=tuple((p...  48 us
    pallas_call x1, Pallas kernels, layer_call(): pl.pallas_call(store_kernel, out_shape=made, in_specs=[anywhere] * 4, out...  2.12 us

profile of v5, /device:TPU:0, one launch (start us, length us, event | category | flops | bytes accessed | tf_op | source)
XLA Modules:
  0.0 50.8 jit_solution(11145503534379580334)
XLA Ops:
  0.6 48.0 %shard_map.228 = (bf16[32,2048]{1,0:T(8,128)(2,1)S(1)}, f32[32,4,64,64]{3,2,1,0:T(8,128)S(1)}, f32[32,4,64]{2,1,0:T(4,128)S(1)}, f32[4,32]{1,0:T(4,128)S(1)}) custom-call(bf16[32,2048]{1,0:T(8,128)(2,1)} %tokens_hbm.1, f32[1,2048]{1,0:T(1,128)} %bitcast.21, bf16[128,256]{1,0:T(8,128)(2,1)} %wq_hbm.1, bf16[128,256]{1,0:T(8,128)(2,1)} %wk_hbm.1, ...), custom_call_target="tpu_custom_call" | custom-call | tf_op jit(solution)/shard_map/pallas_call | solution.py:912
  48.7 2.1 %shard_map.229 = (bf16[32,2048]{1,0:T(8,128)(2,1)}, f32[32,4,64,64]{3,2,1,0:T(8,128)}, f32[32,4,64]{2,1,0:T(4,128)}, f32[4,32]{1,0:T(4,128)}) custom-call(bf16[32,2048]{1,0:T(8,128)(2,1)S(1)} %get-tuple-element.12.mixed_ref, f32[32,4,64,64]{3,2,1,0:T(8,128)S(1)} %get-tuple-element.13.matrix_ref, f32[32,4,64]{2,1,0:T(4,128)S(1)} %get-tuple-element.14.norm_ref, ...), custom_call_target="tpu_custom_call" | custom-call | tf_op jit(solution)/shard_map/pallas_call | solution.py:1010
